TPU v7x, 256 devices: a whole 4x4x8 slice. The times are simulated.
256 devices in a mesh: sp: 64 (over z, y, core), tp: 4 (over x).
Axes of the slice: x: 4, y: 4, z: 8, core: 2. Of those that a mesh axis runs over, the one named last changes fastest.
Arguments:
- out_cotangent: bfloat16 [8192, 2048], P('sp'), may hold values from -16 to 16
- routes: int32 [8192, 2], P('sp'), may hold values from 0 to 63, all different within a row; in each aligned block of 128 rows (0 to 127, 128 to 255, ...) at most 6 rows name the same one
- route_weights: float32 [8192, 2], P('sp'), may hold values from 0.3 to 1.5
- expert_rows: bfloat16 [64, 384, 2048], P('sp', None, 'tp'), may hold values from -6 to 6
- w_gate: bfloat16 [64, 2048, 1024], P('sp', None, 'tp'), may hold values from -0.125 to 0.125
- w_up: bfloat16 [64, 2048, 1024], P('sp', None, 'tp'), may hold values from -0.125 to 0.125
- w_down: bfloat16 [64, 1024, 2048], P('sp', 'tp'), may hold values from -0.1875 to 0.1875
- out_weight: bfloat16 [2048, 4096], P('sp', 'tp'), may hold values from -0.09375 to 0.09375
- values: bfloat16 [8192, 4096], P('sp', 'tp'), may hold values from -0.25 to 0.25
- keys: bfloat16 [8192, 1024], P('sp', 'tp'), may hold values from -0.5 to 0.5
- queries: bfloat16 [8192, 1024], P('sp', 'tp'), may hold values from -6 to 6
- log_decay: float32 [8192, 64], P('sp', 'tp'), may hold values from -1 to 0
- gate_input: bfloat16 [8192, 4096], P('sp', 'tp'), may hold values from -6 to 6
Outputs:
- grad_w_gate: bfloat16 [64, 2048, 1024], P('sp', None, 'tp')
- grad_w_up: bfloat16 [64, 2048, 1024], P('sp', None, 'tp')
- grad_w_down: bfloat16 [64, 1024, 2048], P('sp', 'tp')
- grad_out_weight: float32 [2048, 4096], P('sp', 'tp')
- grad_residual: float32 [8192, 2048], P('sp', 'tp')
- grad_values: float32 [8192, 4096], P('sp', 'tp')
- grad_keys: float32 [8192, 1024], P('sp', 'tp')
- grad_queries: float32 [8192, 1024], P('sp', 'tp')
- grad_decay: float32 [8192, 64], P('sp', 'tp')
- grad_gate: float32 [8192, 4096], P('sp', 'tp')
Inputs may be any that keep to these rules, and one draw needn't show every extreme that they name: `routes`: in each aligned block of 128 tokens no expert is named by more than 6 pairs, a bound that some block reaches.
All inputs are finite; a program needn't handle non-finite values.
Results may differ from a plain program's by a relative error of at most 0.0062.
Values may be sent and summed in bfloat16 or wider, within the bound.
A program may use at most 128 MiB of HBM per device.

v0:
```python
import jax
import jax.numpy as jnp
from jax import lax
from jax.sharding import Mesh
from jax.sharding import PartitionSpec as P

STATE = 128
SPAN = 128
SP = ("sp_0", "sp_1", "sp_2")


HIGHEST = lax.Precision.HIGHEST


def nothing_yet(shard, identity):
    return jax.tree.map(
        lambda part, zero: jnp.zeros_like(part) + jnp.asarray(zero, part.dtype), shard, identity
    )


def carried_in(shard, axes, combine, identity, reverse):
    before = start = nothing_yet(shard, identity)
    running = shard
    for axis in reversed(axes):
        length, here = (lax.axis_size(axis), lax.axis_index(axis))
        pieces = jax.tree.map(lambda part: lax.all_gather(part, axis), running)
        inside, running = (start, start)
        for k in reversed(range(length)) if reverse else range(length):
            passed = k > here if reverse else k < here
            running = combine(running, jax.tree.map(lambda part: part[k], pieces))
            inside = jax.tree.map(lambda new, old: jnp.where(passed, new, old), running, inside)
        before = combine(inside, before)
    return before


def block_step(state_now, block_input):
    values_blk, keys_blk, queries_blk, decay_blk = block_input
    span_len, head_count, head_dim = values_blk.shape
    groups = keys_blk.shape[1]
    state_dim = keys_blk.shape[2]
    repeat = head_count // groups
    cumulative = jnp.cumsum(decay_blk, axis=0)
    lower_mask = jnp.arange(span_len)[:, None] >= jnp.arange(span_len)[None, :]
    segment = cumulative[:, None, :] - cumulative[None, :, :]
    weights = jnp.exp(jnp.where(lower_mask[:, :, None], segment, -jnp.inf)).reshape(
        span_len, span_len, groups, repeat
    )
    inner_prod = jnp.einsum("tgn,sgn->tsg", queries_blk, keys_blk, precision=HIGHEST)
    grouped = values_blk.reshape(span_len, groups, repeat, head_dim)
    combined = inner_prod[:, :, :, None] * weights
    within = jnp.einsum("tsgr,sgrp->tgrp", combined, grouped, precision=HIGHEST)
    carried = jnp.einsum(
        "tgn,grpn->tgrp",
        queries_blk,
        state_now.reshape(groups, repeat, head_dim, state_dim),
        precision=HIGHEST,
    )
    carried = carried * jnp.exp(cumulative).reshape(span_len, groups, repeat)[..., None]
    to_end = jnp.exp(cumulative[-1][None, :] - cumulative).reshape(span_len, groups, repeat)
    added_state = jnp.einsum(
        "sgn,sgrp->grpn", keys_blk, grouped * to_end[..., None], precision=HIGHEST
    )
    new_state = state_now * jnp.exp(cumulative[-1])[:, None, None] + added_state.reshape(
        head_count, head_dim, state_dim
    )
    return (new_state, (within + carried).reshape(span_len, head_count * head_dim))


def mixer_scan(value_f, key_f, query_f, decay_f, start_state):
    row_count = value_f.shape[0]
    head_count = decay_f.shape[1]
    groups = key_f.shape[1] // STATE
    head_dim = value_f.shape[1] // head_count
    span_len = min(SPAN, row_count)
    blocks = row_count // span_len
    value_b = value_f.reshape(blocks, span_len, head_count, head_dim)
    key_b = key_f.reshape(blocks, span_len, groups, STATE)
    query_b = query_f.reshape(blocks, span_len, groups, STATE)
    decay_b = decay_f.reshape(blocks, span_len, head_count)
    end_state, outputs = lax.scan(block_step, start_state, (value_b, key_b, query_b, decay_b))
    return (outputs.reshape(row_count, head_count * head_dim), end_state)


def carry_combine(earlier, later):
    return (earlier[0] * later[0], later[0][:, None, None] * earlier[1] + later[1])


def shards(
    out_cotangent,
    routes,
    route_weights,
    expert_rows,
    w_gate,
    w_up,
    w_down,
    out_weight,
    values,
    keys,
    queries,
    log_decay,
    gate_input,
):
    sp_size = lax.axis_size(SP)
    tp_size = lax.axis_size("tp")
    tok_count, model_width = out_cotangent.shape
    local_experts = w_gate.shape[0]
    slot_count = expert_rows.shape[1]
    capacity = slot_count // sp_size
    experts_all = local_experts * sp_size
    columns = model_width // tp_size
    pair_list = routes.reshape(-1)
    onehot = (pair_list[:, None] == jnp.arange(experts_all, dtype=jnp.int32)[None, :]).astype(
        jnp.int32
    )
    pair_rank = jnp.sum(jnp.cumsum(onehot, axis=0) * onehot, axis=1) - 1
    target = pair_list * capacity + pair_rank
    cotangent_part = lax.dynamic_slice_in_dim(
        out_cotangent, lax.axis_index("tp") * columns, columns, 1
    )
    scaled = (route_weights[:, :, None] * cotangent_part[:, None, :].astype(jnp.float32)).astype(
        jnp.bfloat16
    )
    outgoing = (
        jnp.zeros((experts_all * capacity, columns), jnp.bfloat16)
        .at[target]
        .set(scaled.reshape(-1, columns))
    )
    arrived_part = lax.all_to_all(
        outgoing.reshape(experts_all, capacity, columns),
        SP,
        split_axis=0,
        concat_axis=0,
        tiled=True,
    )
    arrived_part = jnp.moveaxis(
        arrived_part.reshape(sp_size, local_experts, capacity, columns), 0, 1
    )
    arrived_part = arrived_part.reshape(local_experts, slot_count, columns)
    arrived = lax.all_gather(arrived_part, "tp", axis=2, tiled=True)
    full_rows = lax.all_gather(expert_rows, "tp", axis=2, tiled=True)
    gate_pre = jnp.einsum("esd,edf->esf", full_rows, w_gate, preferred_element_type=jnp.float32)
    up_pre = jnp.einsum("esd,edf->esf", full_rows, w_up, preferred_element_type=jnp.float32)
    sigmoid_gate = jax.nn.sigmoid(gate_pre)
    activated = gate_pre * sigmoid_gate
    hidden = (activated * up_pre).astype(jnp.bfloat16)
    hidden_grad = jnp.einsum("esd,efd->esf", arrived, w_down, preferred_element_type=jnp.float32)
    slope = sigmoid_gate * (1.0 + gate_pre * (1.0 - sigmoid_gate))
    gate_grad = (hidden_grad * up_pre * slope).astype(jnp.bfloat16)
    up_grad = (hidden_grad * activated).astype(jnp.bfloat16)
    grad_w_down = jnp.einsum(
        "esf,esd->efd", hidden, arrived, preferred_element_type=jnp.float32
    ).astype(jnp.bfloat16)
    grad_w_gate = jnp.einsum(
        "esd,esf->edf", full_rows, gate_grad, preferred_element_type=jnp.float32
    ).astype(jnp.bfloat16)
    grad_w_up = jnp.einsum(
        "esd,esf->edf", full_rows, up_grad, preferred_element_type=jnp.float32
    ).astype(jnp.bfloat16)
    partial_value = jnp.einsum(
        "esf,edf->esd", gate_grad, w_gate, preferred_element_type=jnp.float32
    )
    partial_value = partial_value + jnp.einsum(
        "esf,edf->esd", up_grad, w_up, preferred_element_type=jnp.float32
    )
    summed = lax.psum_scatter(partial_value, "tp", scatter_dimension=2, tiled=True).astype(
        jnp.bfloat16
    )
    send_back = jnp.moveaxis(summed.reshape(local_experts, sp_size, capacity, columns), 1, 0)
    send_back = send_back.reshape(experts_all, capacity, columns)
    returned = lax.all_to_all(send_back, SP, split_axis=0, concat_axis=0, tiled=True)
    picked = returned.reshape(experts_all * capacity, columns)[target].reshape(
        tok_count, -1, columns
    )
    own_columns = lax.dynamic_slice_in_dim(
        out_cotangent, lax.axis_index("tp") * columns, columns, 1
    )
    grad_residual = own_columns.astype(jnp.float32) + jnp.sum(picked.astype(jnp.float32), axis=1)
    residual_low = lax.all_gather(grad_residual.astype(jnp.bfloat16), "tp", axis=1, tiled=True)
    head_count = log_decay.shape[1]
    groups = keys.shape[1] // STATE
    head_dim = values.shape[1] // head_count
    repeat = head_count // groups
    value_f = values.astype(jnp.float32)
    key_f = keys.astype(jnp.float32)
    query_f = queries.astype(jnp.float32)
    cumulative = jnp.cumsum(log_decay, axis=0)
    decay_total = jnp.exp(cumulative[-1])
    to_end = jnp.exp(cumulative[-1][None, :] - cumulative)
    scaled_values = (value_f.reshape(tok_count, head_count, head_dim) * to_end[:, :, None]).reshape(
        tok_count, groups, repeat, head_dim
    )
    own_state = jnp.einsum(
        "sgn,sgrp->grpn", key_f.reshape(tok_count, groups, STATE), scaled_values, precision=HIGHEST
    )
    own_state = own_state.reshape(head_count, head_dim, STATE)
    identity = (
        jnp.ones((head_count,), jnp.float32),
        jnp.zeros((head_count, head_dim, STATE), jnp.float32),
    )
    entry_state = carried_in((decay_total, own_state), SP, carry_combine, identity, False)[1]
    (mixer_y, leaving), pull_back = jax.vjp(
        mixer_scan, value_f, key_f, query_f, log_decay, entry_state
    )
    part_rows = residual_low
    mixed_grad = jnp.dot(
        part_rows,
        lax.all_gather(out_weight, SP, axis=0, tiled=True),
        preferred_element_type=jnp.float32,
    )
    gate_f = gate_input.astype(jnp.float32)
    gate_sigmoid = jax.nn.sigmoid(gate_f)
    gate_active = gate_f * gate_sigmoid
    gate_slope = gate_sigmoid * (1.0 + gate_f * (1.0 - gate_sigmoid))
    mixed = (mixer_y * gate_active).astype(jnp.bfloat16)
    grad_gate = mixed_grad * mixer_y * gate_slope
    y_grad = mixed_grad * gate_active
    weighted_grad = (
        y_grad.reshape(tok_count, head_count, head_dim) * jnp.exp(cumulative)[:, :, None]
    ).reshape(tok_count, groups, repeat, head_dim)
    reached_state = jnp.einsum(
        "tgn,tgrp->grpn",
        query_f.reshape(tok_count, groups, STATE),
        weighted_grad,
        precision=HIGHEST,
    )
    reached_state = reached_state.reshape(head_count, head_dim, STATE)
    later_state = carried_in((decay_total, reached_state), SP, carry_combine, identity, True)[1]
    grad_values, grad_keys, grad_queries, grad_decay, unused_state = pull_back(
        (y_grad, later_state)
    )
    part_rows = residual_low
    grad_out_weight = lax.psum_scatter(
        lax.dot_general(
            part_rows, mixed, (((0,), (0,)), ((), ())), preferred_element_type=jnp.float32
        ),
        SP,
        scatter_dimension=0,
        tiled=True,
    )
    return (
        grad_w_gate,
        grad_w_up,
        grad_w_down,
        grad_out_weight,
        grad_residual,
        grad_values,
        grad_keys,
        grad_queries,
        grad_decay,
        grad_gate,
    )


def solution(mesh):
    finer = Mesh(mesh.devices.reshape(8, 4, 2, mesh.shape["tp"]), ("sp_0", "sp_1", "sp_2", "tp"))
    in_specs = (
        P(SP, None),
        P(SP, None),
        P(SP, None),
        P(SP, None, "tp"),
        P(SP, None, "tp"),
        P(SP, None, "tp"),
        P(SP, "tp", None),
        P(SP, "tp"),
        P(SP, "tp"),
        P(SP, "tp"),
        P(SP, "tp"),
        P(SP, "tp"),
        P(SP, "tp"),
    )
    out_specs = (
        P(SP, None, "tp"),
        P(SP, None, "tp"),
        P(SP, "tp", None),
        P(SP, "tp"),
        P(SP, "tp"),
        P(SP, "tp"),
        P(SP, "tp"),
        P(SP, "tp"),
        P(SP, "tp"),
        P(SP, "tp"),
    )
    return jax.shard_map(
        shards, mesh=finer, in_specs=in_specs, out_specs=out_specs, check_vma=False
    )
```

profile of v0, /device:TPU:1, one launch (start us, length us, event | category | flops | bytes accessed | tf_op | source)
XLA Modules:
  0.0 568.7 jit_solution(100809377200915807)
XLA Ops:
  8.8 0.8 copy.79
  11.7 0.8 copy.82
  12.6 0.9 dynamic-slice_convert_fusion
  14.2 1.7 scatter_custom_fusion
  16.1 30.6 %all_to_all.10 = bf16[64,6,512]{2,1,0:T(8,128)(2,1)S(1)} all-to-all(bf16[64,6,512]{2,1,0:T(8,128)(2,1)S(1)} %reshape.691), channel_id=1, replica_groups=mesh['sp_0'=8,'sp_1'=4,'sp_2'=2,'tp'=4] {'sp_0','sp_1','sp_2'}, dimensions={0} | all-to-all | bytes 786432 | tf_op jit(solution)/shard_map/all_to_all | solution.py:128
  46.7 0.9 reshape_transpose_reshape.6
  47.7 2.1 fusion.5
  49.8 1.9 fusion.7
  51.8 22.9 %all-gather.14.cloned.1.call-done = bf16[1,384,2048]{2,1,0:T(8,128)(2,1)} async-done(((bf16[1,384,512]{2,1,0:T(8,128)(2,1)}), bf16[1,384,2048]{2,1,0:T(8,128)(2,1)}) %all-gather.14.cloned.1.call-update) | async-done | bytes 1572880 | tf_op jit(solution)/shard_map/all_gather | solution.py:139
  74.7 2.3 multiply_convert_fusion.3
  78.4 2.2 add_bitcast_fusion
  81.3 40.5 %reduce-scatter.3.cloned.1.call-done = f32[1,384,512]{2,1,0:T(8,128)} async-done(((f32[1,384,2048]{2,1,0:T(8,128)}), f32[1,384,512]{2,1,0:T(8,128)}) %reduce-scatter.3.cloned.1.call-update) | async-done | bytes 786448 | tf_op jit(solution)/shard_map/reduce_scatter | solution.py:165
  121.8 1.2 convert_element_type.85
  123.0 0.9 reshape_transpose_reshape.7
  123.9 10.7 %all-to-all-start.1 = ((bf16[64,6,512]{2,1,0:T(8,128)(2,1)}), bf16[64,6,512]{2,1,0:T(8,128)(2,1)S(1)}, u32[]{:S(2)}, u32[]{:S(2)}) async-start(bf16[64,6,512]{2,1,0:T(8,128)(2,1)} %reshape_transpose_reshape.7), calls=%async_computation.2 | async-start | bytes 1048576 | tf_op jit(solution)/shard_map/all_to_all | solution.py:170
  135.1 21.1 %all-to-all-done.1 = bf16[64,6,512]{2,1,0:T(8,128)(2,1)S(1)} async-done(((bf16[64,6,512]{2,1,0:T(8,128)(2,1)}), bf16[64,6,512]{2,1,0:T(8,128)(2,1)S(1)}, u32[]{:S(2)}, u32[]{:S(2)}) %all-to-all-start.1) | async-done | bytes 393248 | tf_op jit(solution)/shard_map/all_to_all | solution.py:170
  156.4 1.2 gather_fusion
  158.5 1.7 fusion.99
  160.2 10.3 %all_gather.56 = bf16[128,2048]{1,0:T(8,128)(2,1)S(1)} all-gather(bf16[128,512]{1,0:T(8,128)(2,1)S(1)} %get-tuple-element.222), channel_id=1, replica_groups=mesh['sp_0'=8,'sp_1'=4,'sp_2'=2,'tp'=4] {'tp'}, dimensions={1}, use_global_device_ids=true | all-gather | bytes 655360 | tf_op jit(solution)/shard_map/all_gather | solution.py:178
  170.5 4.0 fusion.72
  174.7 1.2 fusion.62
  176.5 4.2 all-gather
  181.2 8.4 %all-gather.1 = f32[4,1,16]{2,1,0:T(1,128)S(1)} all-gather(f32[1,1,16]{2,1,0:T(1,128)S(1)} %get-tuple-element.301), channel_id=1, replica_groups=mesh['sp_0'=8,'sp_1'=4,'sp_2'=2,'tp'=4] {'sp_1'}, dimensions={0}, use_global_device_ids=true | all-gather | bytes 320 | tf_op jit(solution)/shard_map/all_gather | solution.py:26
  190.2 2.3 multiply_add_fusion.1
  193.2 31.9 %all-gather.28.cloned.1.call-done = f32[4,16,64,128]{3,2,1,0:T(8,128)} async-done(((f32[1,16,64,128]{3,2,1,0:T(8,128)}), f32[4,16,64,128]{3,2,1,0:T(8,128)}) %all-gather.28.cloned.1.call-update) | async-done | bytes 2097168 | tf_op jit(solution)/shard_map/all_gather | solution.py:26
  225.1 3.3 multiply_add_fusion
  230.2 12.8 %all-gather.3 = f32[8,1,16]{2,1,0:T(1,128)S(1)} all-gather(f32[1,1,16]{2,1,0:T(1,128)S(1)} %get-tuple-element.282), channel_id=1, replica_groups=mesh['sp_0'=8,'sp_1'=4,'sp_2'=2,'tp'=4] {'sp_0'}, dimensions={0}, use_global_device_ids=true | all-gather | bytes 576 | tf_op jit(solution)/shard_map/all_gather | solution.py:26
  249.6 33.8 %all-gather.30.cloned.1.call-done = f32[8,16,64,128]{3,2,1,0:T(8,128)} async-done(((f32[1,16,64,128]{3,2,1,0:T(8,128)}), f32[8,16,64,128]{3,2,1,0:T(8,128)}) %all-gather.30.cloned.1.call-update) | async-done | bytes 4194320 | tf_op jit(solution)/shard_map/all_gather | solution.py:26
  283.6 2.6 fusion.102
  286.5 2.6 add_add_fusion
  289.1 1.2 fusion.27
  290.3 0.7 multiply_reduce_fusion.2
  291.0 1.2 fusion.26
  292.2 13.8 %all-gather.18.cloned.1.call-done = f32[2,16,64,128]{3,2,1,0:T(8,128)} async-done(((f32[1,16,64,128]{3,2,1,0:T(8,128)}), f32[2,16,64,128]{3,2,1,0:T(8,128)}) %all-gather.18.cloned.1.call-update) | async-done | bytes 1048592 | tf_op jit(solution)/shard_map/all_gather | solution.py:26
  306.0 2.4 multiply_add_fusion.3
  308.6 33.6 %all-gather.20.cloned.1.call-done = f32[4,16,64,128]{3,2,1,0:T(8,128)} async-done(((f32[1,16,64,128]{3,2,1,0:T(8,128)}), f32[4,16,64,128]{3,2,1,0:T(8,128)}) %all-gather.20.cloned.1.call-update) | async-done | bytes 2097168 | tf_op jit(solution)/shard_map/all_gather | solution.py:26
  342.2 3.2 multiply_add_fusion.2
  345.8 12.8 %all-gather.2 = f32[8,1,16]{2,1,0:T(1,128)S(1)} all-gather(f32[1,1,16]{2,1,0:T(1,128)S(1)} %copy-done.91), channel_id=1, replica_groups=mesh['sp_0'=8,'sp_1'=4,'sp_2'=2,'tp'=4] {'sp_0'}, dimensions={0}, use_global_device_ids=true | all-gather | bytes 576 | tf_op jit(solution)/shard_map/all_gather | solution.py:26
  364.7 0.8 copy.85
  366.1 34.4 %all-gather.22.cloned.1.call-done = f32[8,16,64,128]{3,2,1,0:T(8,128)} async-done(((f32[1,16,64,128]{3,2,1,0:T(8,128)}), f32[8,16,64,128]{3,2,1,0:T(8,128)}) %all-gather.22.cloned.1.call-update) | async-done | bytes 4194320 | tf_op jit(solution)/shard_map/all_gather | solution.py:26
  400.6 2.6 fusion.101
  403.7 1.4 add_add_fusion.1
  405.2 1.0 multiply_reduce_fusion.1
  406.2 2.1 fusion.13
  408.3 1.2 copy.91
  409.6 5.9 %fusion.66 = f32[2048,1024]{1,0:T(8,128)} fusion(bf16[128,2048]{1,0:T(8,128)(2,1)} %copy-done.7, f32[128,1024]{1,0:T(8,128)S(1)} %copy.91, bf16[128,1024]{1,0:T(8,128)(2,1)} %param.25), kind=kOutput, calls=%fused_computation.129 | convolution fusion | flops 537788416 | bytes 9699328 | tf_op jit(solution)/shard_map/dot_general | solution.py:233
  416.7 1.7 fusion
  418.4 2.3 copy.104
  420.7 1.7 fusion.1
  422.4 2.4 copy.105
  424.8 2.8 fusion.2
  427.6 1.5 fusion.25
  429.2 0.7 copy.101
  430.5 1.0 convolution_bitcast_fusion.6
  431.8 0.8 copy.107
  432.6 3.3 fusion.12
  435.9 2.1 copy.106
  438.1 1.0 convolution_bitcast_fusion.5
  439.4 0.8 copy.108
  440.2 0.7 copy.100
  441.0 6.8 %fusion.38 = f32[16]{0:T(128)S(1)} fusion(f32[16]{0:T(128)} %copy-done.73, f32[16]{0:T(128)S(1)} %copy-done.69, f32[16]{0:T(128)} %copy-done.70, f32[16]{0:T(128)} %copy-done.75, f32[16]{0:T(128)} %get-tuple-element.215, f32[16]{0:T(128)} %get-tuple-element.278, f32[16]{0:T(128)} %get-tuple-element.277, f32[16]{0:T(128)} %get-tuple-element.276, ...), kind=kLoop, calls=%fused_computation.61 | loop fusion | flops 11534320 | bytes 14682076 | tf_op jit(solution)/shard_map/transpose(jvp())/while/body/eval_jaxpr/reduce_sum | solution.py:63
  447.9 1.1 reduce_window_sum.44
  449.6 2.2 fusion.33
  451.9 109.7 %reduce-scatter.5.cloned.1.call-done = f32[32,1024]{1,0:T(8,128)} async-done(((f32[2048,1024]{1,0:T(8,128)}), f32[32,1024]{1,0:T(8,128)}) %reduce-scatter.5.cloned.1.call-update) | async-done | bytes 131088 | tf_op jit(solution)/shard_map/reduce_scatter | solution.py:232
  (322 shorter events, 29.3 us)
Async XLA Ops:
  8.0 39.7 %copy-start = (bf16[1,2048,256]{2,1,0:T(8,128)(2,1)S(1)}, bf16[1,2048,256]{2,1,0:T(8,128)(2,1)}, u32[]{:S(2)}) copy-start(bf16[1,2048,256]{2,1,0:T(8,128)(2,1)} %param.17) | copy-start | bytes 3145732
  8.0 39.6 %all-gather.16.cloned.1.call-start = ((), (), s32[]{:S(2)}) async-start(), calls=%async_computation.5 | async-start | bytes 1966080 | tf_op jit(solution)/shard_map/all_gather | solution.py:140
  8.8 65.9 %all-gather.14.cloned.1.call-start = ((), (), s32[]{:S(2)}) async-start(), calls=%async_computation.4 | async-start | bytes 1966080 | tf_op jit(solution)/shard_map/all_gather | solution.py:139
  47.6 74.2 %reduce-scatter.3.cloned.1.call-start = ((), (), s32[]{:S(2)}) async-start(), calls=%async_computation.6 | async-start | bytes 3932160 | tf_op jit(solution)/shard_map/reduce_scatter | solution.py:165
  49.8 27.2 %copy-start.35 = (f32[384,256]{1,0:T(8,128)}, f32[384,256]{1,0:T(8,128)S(1)}, u32[]{:S(2)}) copy-start(f32[384,256]{1,0:T(8,128)S(1)} %fusion.5) | copy-start | bytes 1179652
  51.8 25.3 %copy-start.37 = (f32[384,256]{1,0:T(8,128)}, f32[384,256]{1,0:T(8,128)S(1)}, u32[]{:S(2)}) copy-start(f32[384,256]{1,0:T(8,128)S(1)} %fusion.7) | copy-start | bytes 1179652
  80.7 54.0 %copy-start.48 = (bf16[128,256]{1,0:T(8,128)(2,1)S(1)}, bf16[128,256]{1,0:T(8,128)(2,1)}, u32[]{:S(2)}) copy-start(bf16[128,256]{1,0:T(8,128)(2,1)} %param.23) | copy-start | bytes 196612
  80.7 54.0 %copy-start.65 = (f32[128,16]{0,1:T(8,128)S(1)}, f32[128,16]{0,1:T(8,128)}, u32[]{:S(2)}) copy-start(f32[128,16]{0,1:T(8,128)} %param.24) | copy-start | bytes 24580
  80.7 89.8 %all-gather.24.cloned.1.call-start = ((), (), s32[]{:S(2)}) async-start(), calls=%async_computation.11 | async-start | bytes 4259840 | tf_op jit(solution)/shard_map/all_gather | solution.py:207
  123.9 32.4 %all-to-all-start.1 = ((bf16[64,6,512]{2,1,0:T(8,128)(2,1)}), bf16[64,6,512]{2,1,0:T(8,128)(2,1)S(1)}, u32[]{:S(2)}, u32[]{:S(2)}) async-start(bf16[64,6,512]{2,1,0:T(8,128)(2,1)} %reshape_transpose_reshape.7), calls=%async_computation.2 | async-start | bytes 1048576 | tf_op jit(solution)/shard_map/all_to_all | solution.py:170
  134.6 55.6 %all-gather.26.cloned.1.call-start = ((), (), s32[]{:S(2)}) async-start(), calls=%async_computation.12 | async-start | bytes 1572864 | tf_op jit(solution)/shard_map/all_gather | solution.py:26
  135.0 40.9 %copy-start.27 = (f32[128,16]{1,0:T(8,128)}, f32[128,16]{1,0:T(8,128)S(1)}, u32[]{:S(2)}) copy-start(f32[128,16]{1,0:T(8,128)S(1)} %reduce_window_sum.43) | copy-start | bytes 24580
  135.1 39.6 %copy-start.41 = (f32[128,2,8]{0,2,1:T(8,128)}, f32[128,2,8]{0,2,1:T(8,128)S(1)}, u32[]{:S(2)}) copy-start(f32[128,2,8]{0,2,1:T(8,128)S(1)} %bitcast_exponential_fusion) | copy-start | bytes 24580
  157.5 12.9 %copy-start.20 = (bf16[128,1024]{1,0:T(8,128)(2,1)S(1)}, bf16[128,1024]{1,0:T(8,128)(2,1)}, u32[]{:S(2)}) copy-start(bf16[128,1024]{1,0:T(8,128)(2,1)} %param.25) | copy-start | bytes 786436
  170.5 4.0 copy-start.7
  175.9 49.2 %all-gather.28.cloned.1.call-start = ((), (), s32[]{:S(2)}) async-start(), calls=%async_computation.13 | async-start | bytes 2621440 | tf_op jit(solution)/shard_map/all_gather | solution.py:26
  180.6 47.7 %copy-start.57 = (f32[2,1,16]{2,1,0:T(1,128)}, f32[2,1,16]{2,1,0:T(1,128)S(1)}, u32[]{:S(2)}) copy-start(f32[2,1,16]{2,1,0:T(1,128)S(1)} %all-gather) | copy-start | bytes 388
  181.2 11.3 %copy-start.68 = (f32[16]{0:T(128)}, f32[16]{0:T(128)S(1)}, u32[]{:S(2)}) copy-start(f32[16]{0:T(128)S(1)} %get-tuple-element.298) | copy-start | bytes 196
  189.6 40.0 %copy-start.50 = (f32[4,1,16]{2,1,0:T(1,128)}, f32[4,1,16]{2,1,0:T(1,128)S(1)}, u32[]{:S(2)}) copy-start(f32[4,1,16]{2,1,0:T(1,128)S(1)} %all-gather.1) | copy-start | bytes 772
  190.2 38.1 %copy-start.70 = (f32[16]{0:T(128)}, f32[16]{0:T(128)S(1)}, u32[]{:S(2)}) copy-start(f32[16]{0:T(128)S(1)} %get-tuple-element.279) | copy-start | bytes 196
  192.5 90.9 %all-gather.30.cloned.1.call-start = ((), (), s32[]{:S(2)}) async-start(), calls=%async_computation.14 | async-start | bytes 4718592 | tf_op jit(solution)/shard_map/all_gather | solution.py:26
  193.2 35.2 %copy-start.59 = (f32[16]{0:T(128)}, f32[16]{0:T(128)S(1)}, u32[]{:S(2)}) copy-start(f32[16]{0:T(128)S(1)} %get-tuple-element.284) | copy-start | bytes 196
  193.2 35.2 %copy-start.62 = (f32[16]{0:T(128)}, f32[16]{0:T(128)S(1)}, u32[]{:S(2)}) copy-start(f32[16]{0:T(128)S(1)} %get-tuple-element.286) | copy-start | bytes 196
  193.2 35.2 %copy-start.75 = (f32[16]{0:T(128)}, f32[16]{0:T(128)S(1)}, u32[]{:S(2)}) copy-start(f32[16]{0:T(128)S(1)} %get-tuple-element.285) | copy-start | bytes 196
  225.0 23.8 %copy-start.38 = (bf16[128,1024]{1,0:T(8,128)(2,1)S(1)}, bf16[128,1024]{1,0:T(8,128)(2,1)}, u32[]{:S(2)}) copy-start(bf16[128,1024]{1,0:T(8,128)(2,1)} %param.21) | copy-start | bytes 786436
  228.4 77.7 %all-gather.18.cloned.1.call-start = ((), (), s32[]{:S(2)}) async-start(), calls=%async_computation.7 | async-start | bytes 1572864 | tf_op jit(solution)/shard_map/all_gather | solution.py:26
  229.2 57.0 %copy-start.84 = (f32[2,8]{1,0:T(2,128)}, f32[2,8]{1,0:T(2,128)S(1)}, u32[]{:S(2)}) copy-start(f32[2,8]{1,0:T(2,128)S(1)} %squeeze.234) | copy-start | bytes 196
  229.3 56.9 %copy-start.76 = (f32[2,8]{1,0:T(2,128)}, f32[2,8]{1,0:T(2,128)S(1)}, u32[]{:S(2)}) copy-start(f32[2,8]{1,0:T(2,128)S(1)} %squeeze.235) | copy-start | bytes 196
  229.3 56.8 %copy-start.85 = (f32[2,8]{1,0:T(2,128)}, f32[2,8]{1,0:T(2,128)S(1)}, u32[]{:S(2)}) copy-start(f32[2,8]{1,0:T(2,128)S(1)} %squeeze.230) | copy-start | bytes 196
  229.4 56.8 %copy-start.53 = (f32[2,8]{1,0:T(2,128)}, f32[2,8]{1,0:T(2,128)S(1)}, u32[]{:S(2)}) copy-start(f32[2,8]{1,0:T(2,128)S(1)} %squeeze.231) | copy-start | bytes 196
  229.5 56.7 %copy-start.55 = (f32[2,8]{1,0:T(2,128)}, f32[2,8]{1,0:T(2,128)S(1)}, u32[]{:S(2)}) copy-start(f32[2,8]{1,0:T(2,128)S(1)} %squeeze.232) | copy-start | bytes 196
  229.6 56.6 %copy-start.78 = (f32[2,8]{1,0:T(2,128)}, f32[2,8]{1,0:T(2,128)S(1)}, u32[]{:S(2)}) copy-start(f32[2,8]{1,0:T(2,128)S(1)} %squeeze.233) | copy-start | bytes 196
  286.4 3.8 copy-start.109
  289.1 17.0 %copy-start.66 = (f32[16]{0:T(128)S(1)}, f32[16]{0:T(128)}, u32[]{:S(2)}) copy-start(f32[16]{0:T(128)} %get-tuple-element.297) | copy-start | bytes 196
  289.1 17.0 %copy-start.72 = (f32[16]{0:T(128)S(1)}, f32[16]{0:T(128)}, u32[]{:S(2)}) copy-start(f32[16]{0:T(128)} %get-tuple-element.291) | copy-start | bytes 196
  290.3 18.2 %copy-start.44 = (f32[128,2,8]{0,2,1:T(8,128)}, f32[128,2,8]{0,2,1:T(8,128)S(1)}, u32[]{:S(2)}) copy-start(f32[128,2,8]{0,2,1:T(8,128)S(1)} %get-tuple-element.304) | copy-start | bytes 24580
  291.0 51.2 %copy-start.60 = (f32[16]{0:T(128)S(1)}, f32[16]{0:T(128)}, u32[]{:S(2)}) copy-start(f32[16]{0:T(128)} %copy-done.59) | copy-start | bytes 196
  291.0 51.2 %copy-start.63 = (f32[16]{0:T(128)S(1)}, f32[16]{0:T(128)}, u32[]{:S(2)}) copy-start(f32[16]{0:T(128)} %copy-done.62) | copy-start | bytes 196
  291.0 51.2 %copy-start.71 = (f32[16]{0:T(128)S(1)}, f32[16]{0:T(128)}, u32[]{:S(2)}) copy-start(f32[16]{0:T(128)} %get-tuple-element.280) | copy-start | bytes 196
  291.0 51.2 %copy-start.74 = (f32[16]{0:T(128)S(1)}, f32[16]{0:T(128)}, u32[]{:S(2)}) copy-start(f32[16]{0:T(128)} %get-tuple-element.283) | copy-start | bytes 196
  292.2 50.0 %all-gather.20.cloned.1.call-start = ((), (), s32[]{:S(2)}) async-start(), calls=%async_computation.8 | async-start | bytes 2621440 | tf_op jit(solution)/shard_map/all_gather | solution.py:26
  308.5 92.0 %all-gather.22.cloned.1.call-start = ((), (), s32[]{:S(2)}) async-start(), calls=%async_computation.9 | async-start | bytes 4718592 | tf_op jit(solution)/shard_map/all_gather | solution.py:26
  345.5 216.1 %reduce-scatter.5.cloned.1.call-start = ((), (), s32[]{:S(2)}) async-start(), calls=%async_computation.10 | async-start | bytes 8519680 | tf_op jit(solution)/shard_map/reduce_scatter | solution.py:232
  345.7 57.6 %copy-start.29 = (bf16[128,2,128]{0,2,1:T(8,128)(2,1)}, bf16[128,2,128]{0,2,1:T(8,128)(2,1)S(1)}, u32[]{:S(2)}) copy-start(bf16[128,2,128]{0,2,1:T(8,128)(2,1)S(1)} %copy.98) | copy-start | bytes 196612
  409.6 5.9 %copy-start.4 = (f32[128,1024]{1,0:T(8,128)}, f32[128,1024]{1,0:T(8,128)S(1)}, u32[]{:S(2)}) copy-start(f32[128,1024]{1,0:T(8,128)S(1)} %copy.91) | copy-start | bytes 1572868
  416.7 4.0 copy-start.26
  430.5 7.5 %copy-start.6 = (f32[2,8,64,128]{3,2,1,0:T(8,128)S(1)}, f32[2,8,64,128]{3,2,1,0:T(8,128)}, u32[]{:S(2)}) copy-start(f32[2,8,64,128]{3,2,1,0:T(8,128)} %copy-done.5) | copy-start | bytes 1572868
  431.5 6.4 %copy-start.45 = (f32[128,2,8]{0,2,1:T(8,128)S(1)}, f32[128,2,8]{0,2,1:T(8,128)}, u32[]{:S(2)}) copy-start(f32[128,2,8]{0,2,1:T(8,128)} %copy-done.44) | copy-start | bytes 24580
  431.6 6.5 %copy-start.43 = (f32[128,2,8]{0,2,1:T(8,128)S(1)}, f32[128,2,8]{0,2,1:T(8,128)}, u32[]{:S(2)}) copy-start(f32[128,2,8]{0,2,1:T(8,128)} %copy-done.41) | copy-start | bytes 24580
  431.8 7.3 %copy-start.30 = (bf16[128,2,128]{0,2,1:T(8,128)(2,1)S(1)}, bf16[128,2,128]{0,2,1:T(8,128)(2,1)}, u32[]{:S(2)}) copy-start(bf16[128,2,128]{0,2,1:T(8,128)(2,1)} %copy-done.29) | copy-start | bytes 196612
  432.6 6.6 %copy-start.32 = (f32[128,128,2]{1,0,2:T(8,128)S(1)}, f32[128,128,2]{1,0,2:T(8,128)}, u32[]{:S(2)}) copy-start(f32[128,128,2]{1,0,2:T(8,128)} %copy-done.31) | copy-start | bytes 393220
  432.6 7.6 %copy-start.52 = (f32[128,2,8]{0,2,1:T(8,128)S(1)}, f32[128,2,8]{0,2,1:T(8,128)}, u32[]{:S(2)}) copy-start(f32[128,2,8]{0,2,1:T(8,128)} %get-tuple-element.306) | copy-start | bytes 24580
  432.6 8.3 %copy-start.2 = (f32[4,16,64,128]{3,2,1,0:T(8,128)S(1)}, f32[4,16,64,128]{3,2,1,0:T(8,128)}, u32[]{:S(2)}) copy-start(f32[4,16,64,128]{3,2,1,0:T(8,128)} %all-gather.28.cloned.1.call-done) | copy-start | bytes 6291460
  435.9 5.0 copy-start.61
  435.9 5.0 copy-start.64
  435.9 5.0 copy-start.67
  435.9 5.0 copy-start.69
  440.9 6.8 %copy-start.28 = (f32[128,16]{1,0:T(8,128)S(1)}, f32[128,16]{1,0:T(8,128)}, u32[]{:S(2)}) copy-start(f32[128,16]{1,0:T(8,128)} %copy-done.27) | copy-start | bytes 24580
  440.9 6.9 %copy-start.39 = (f32[128,16]{1,0:T(8,128)S(1)}, f32[128,16]{1,0:T(8,128)}, u32[]{:S(2)}) copy-start(f32[128,16]{1,0:T(8,128)} %copy.101) | copy-start | bytes 24580
  440.9 6.9 %copy-start.40 = (f32[128,16]{1,0:T(8,128)S(1)}, f32[128,16]{1,0:T(8,128)}, u32[]{:S(2)}) copy-start(f32[128,16]{1,0:T(8,128)} %copy.100) | copy-start | bytes 24580
  440.9 6.9 %copy-start.90 = (f32[16]{0:T(128)S(1)}, f32[16]{0:T(128)}, u32[]{:S(2)}) copy-start(f32[16]{0:T(128)} %get-tuple-element.258) | copy-start | bytes 196
  441.0 6.9 %copy-start.110 = (f32[1,16]{1,0:T(1,128)S(1)}, f32[1,16]{1,0:T(1,128)}, u32[]{:S(2)}) copy-start(f32[1,16]{1,0:T(1,128)} %reshape.706) | copy-start | bytes 196
  441.0 8.7 %copy-start.21 = (bf16[128,1024]{1,0:T(8,128)(2,1)S(1)}, bf16[128,1024]{1,0:T(8,128)(2,1)}, u32[]{:S(2)}) copy-start(bf16[128,1024]{1,0:T(8,128)(2,1)} %param.25) | copy-start | bytes 786436
  441.0 120.6 %copy-start.1 = (bf16[1,2048,256]{2,1,0:T(8,128)(2,1)S(1)}, bf16[1,2048,256]{2,1,0:T(8,128)(2,1)}, u32[]{:S(2)}) copy-start(bf16[1,2048,256]{2,1,0:T(8,128)(2,1)} %param.17) | copy-start | bytes 3145732
  (59 other events, 158.7 us)
Sparse Core Ops, SparseCore 0:
  10.6 32.5 all-gather.15
  47.7 26.9 all-gather.13
  80.8 40.9 reduce-scatter.2
  228.5 54.8 all-gather.29
  345.6 54.8 all-gather.21
Sparse Core Ops, SparseCore 1:
  84.0 83.1 all-gather.23
  176.0 13.0 all-gather.25
  192.6 32.4 all-gather.27
  292.3 13.7 all-gather.17
  308.6 33.6 all-gather.19
  415.6 145.9 reduce-scatter.4
where the time goes:
time: 574 us; the launch traced here: 569 us
  waiting for transfers between devices  343 us (60%)
  blocking collectives  79.2 us (14%)
  local copies, waits for them, and re-layouts  40.5 us (7%)
  matrix products  39.5 us (7%)
  other arithmetic  38.5 us (7%)
  between operations  16.7 us (3%)
  starting transfers between devices  11.2 us (2%)
    all_gather x6, waiting for transfers between devices, carried_in(): pieces = jax.tree.map(lambda part: lax.all_gather(part, axis), running)  147 us
    reduce_scatter x1, waiting for transfers between devices, shards(): lax.psum_scatter(lax.dot_general(part_rows, mixed, (((0,), (0,)), ((), ()...  110 us
    reduce_scatter x1, waiting for transfers between devices, shards(): lax.psum_scatter(partial_value, 'tp', scatter_dimension=2, tiled=True)  40.5 us
    all_gather x4, blocking collectives, carried_in(): pieces = jax.tree.map(lambda part: lax.all_gather(part, axis), running)  38.2 us
    all_to_all x1, blocking collectives, shards(): lax.all_to_all(outgoing.reshape(experts_all, capacity, columns), SP, spli...  30.6 us
    all_gather x1, waiting for transfers between devices, shards(): arrived = lax.all_gather(arrived_part, 'tp', axis=2, tiled=True)  22.9 us
    all_to_all x1, waiting for transfers between devices, shards(): lax.all_to_all(send_back, SP, split_axis=0, concat_axis=0, tiled=True)  21.1 us
    add x6, other arithmetic, carry_combine(): later[0][:, None, None] * earlier[1] + later[1]  15.2 us
  transfers between devices with their start and end apart: 12, of which 9 were waited for; matrix products, arithmetic and copies ran while one was open for 13% of the time, Pallas kernels for 0%

commit v1 on v0

v1 whole, which is shorter than its diff:
```python
import jax
import jax.numpy as jnp
from jax import lax
from jax.experimental import pallas as pl
from jax.experimental.pallas import tpu as pltpu
from jax.sharding import PartitionSpec as P

MESH = pl.DeviceIdType.MESH
F32, BF16 = jnp.float32, jnp.bfloat16
HIGHEST = lax.Precision.HIGHEST

BUFFERS = dict(
    cot=((128, 512), BF16),
    routes=((2, 128), jnp.int32),
    route_weights=((2, 128), F32),
    w_gate=((2048, 256), BF16),
    w_up=((2048, 256), BF16),
    w_down=((256, 2048), BF16),
    out_weight=((32, 1024), BF16),
    v=((128, 1024), BF16),
    k=((128, 256), BF16),
    q=((128, 256), BF16),
    log_decay=((16, 128), F32),
    gate=((128, 1024), BF16),
    pack_out=((64, 8, 384), BF16),
    pack_in=((64, 8, 384), BF16),
    ret_out=((64, 8, 384), BF16),
    ret_in=((64, 8, 384), BF16),
    hit_a=((2, 128, 512), BF16),
    hit_b=((2, 3, 128, 512), BF16),
    sel_a=((384, 512), BF16),
    sel_b=((3, 384, 512), BF16),
    arr=((4, 384, 512), BF16),
    full=((4, 384, 512), BF16),
    gate_pre=((384, 256), F32),
    up_pre=((384, 256), F32),
    hidden_grad=((384, 256), F32),
    hidden=((384, 256), BF16),
    gate_grad=((384, 256), BF16),
    up_grad=((384, 256), BF16),
    rs_opp=((384, 512), BF16),
    rs_right=((384, 512), BF16),
    rs_left=((384, 512), BF16),
    rs_half_l=((192, 512), BF16),
    rs_half_r=((192, 512), BF16),
    rs_in_l=((384, 512), BF16),
    rs_in_r=((384, 512), BF16),
    rs_own=((384, 512), F32),
    rs_own_l=((384, 512), F32),
    resid=((4, 128, 512), BF16),
    res_t=((8, 8, 32, 128), BF16),
    res_in=((8, 8, 32, 128), BF16),
    weight=((8, 8, 32, 1024), BF16),
    mixed=((8, 128, 1024), BF16),
    gow_part=((8, 32, 1024), F32),
    gow_out=((8, 32, 1024), BF16),
    gow_in=((8, 32, 1024), BF16),
    c_exp=((128, 1024), F32),
    to_end=((128, 1024), F32),
    from_start=((128, 1024), F32),
    c_row=((16, 128), F32),
    c_col=((128, 128), F32),
    v_end=((2, 128, 1024), BF16),
    qk=((2, 128, 128), F32),
    decay=((8, 128, 256), F32),
    score=((2, 8, 128, 256), BF16),
    y=((128, 1024), F32),
    carried=((128, 1024), F32),
    dy=((128, 1024), F32),
    dy_start=((2, 128, 1024), BF16),
    dv=((128, 1024), F32),
    dqk=((2, 128, 128), F32),
    row_col=((128, 128), F32),
    dq=((128, 256), F32),
    log_out=((8, 8, 128), F32),
    log_in=((8, 8, 128), F32),
    log_run=((8, 128), F32),
    log_z=((8, 8, 128), F32),
    log_before=((8, 8, 128), F32),
    before=((8, 128, 128), F32),
    f_own=((8, 128, 128), F32),
    f_in=((8, 128, 128), F32),
    f_run=((128, 128), F32),
    f_z=((8, 128, 128), F32),
    f_back=((8, 128, 128), F32),
    state=((8, 128, 128), F32),
    b_own=((8, 128, 128), F32),
    b_in=((8, 128, 128), F32),
    b_run=((128, 128), BF16),
    b_z=((8, 128, 128), BF16),
    b_back=((8, 128, 128), F32),
    dstate=((8, 128, 128), F32),
)
CHANNELS = dict(
    rows=6,
    arrived=6,
    residual=6,
    dispatch=1,
    back=1,
    scatter=6,
    weight_z=1,
    weight_y=6,
    weight_c=1,
    mixed_y=6,
    mixed_c=1,
    gow_j=1,
    gow_z=1,
    f_j=1,
    f_jlog=1,
    f_z=1,
    f_zlog=1,
    f_back=1,
    b_j=1,
    b_z=1,
    b_back=1,
)
INPUTS = dict(
    h_cot=((128, 2048), BF16),
    h_routes=((2, 128), jnp.int32),
    h_route_weights=((2, 128), F32),
    h_rows=((384, 512), BF16),
    h_w_gate=((2048, 256), BF16),
    h_w_up=((2048, 256), BF16),
    h_w_down=((256, 2048), BF16),
    h_out_weight=((32, 1024), BF16),
    h_v=((128, 1024), BF16),
    h_k=((128, 256), BF16),
    h_q=((128, 256), BF16),
    h_log_decay=((16, 128), F32),
    h_gate=((128, 1024), BF16),
)
OUTPUTS = dict(
    g_gate=((2048, 256), BF16),
    g_up=((2048, 256), BF16),
    g_down=((256, 2048), BF16),
    g_out=((32, 1024), F32),
    g_res=((128, 512), F32),
    g_v=((128, 1024), F32),
    g_k=((128, 256), F32),
    g_q=((128, 256), F32),
    g_decay=((16, 128), F32),
    g_gate_in=((128, 1024), F32),
)


class Refs:
    pass


def dot(a, b, ca=1, cb=0, precision=None):
    return lax.dot_general(
        a, b, (((ca,), (cb,)), ((), ())), precision=precision, preferred_element_type=F32
    )


def iota(shape, dim):
    return lax.broadcasted_iota(jnp.int32, shape, dim)


def hot(cond, dtype=BF16):
    return jnp.where(cond, 1.0, 0.0).astype(dtype)


def split(x):
    high = x.astype(BF16)
    return high, (x - high.astype(F32)).astype(BF16)


def fine_dot(a, b, ca=1, cb=0):
    high, low = split(a)
    return dot(high, b, ca, cb) + dot(low, b, ca, cb)


def sigmoid(x):
    return 1.0 / (1.0 + jnp.exp(-x))


def publish(*refs):
    n = len(OUTPUTS)
    sources, targets, held, sems = refs[:n], refs[n : 2 * n], refs[2 * n : 3 * n], refs[3 * n]
    loads = [pltpu.make_async_copy(sources[i], held[i], sems.at[0, i]) for i in range(n)]
    stores = [pltpu.make_async_copy(held[i], targets[i], sems.at[1, i]) for i in range(n)]
    for load in loads:
        load.start()
    for load, store in zip(loads, stores):
        load.wait()
        store.start()
    for store in stores:
        store.wait()


def kernel(*refs):
    r, c, local, result = Refs(), Refs(), Refs(), Refs()
    names = list(INPUTS) + list(OUTPUTS) + list(BUFFERS)
    for name, ref in zip(names, refs):
        setattr(r, name, ref)
    at = len(names)
    for name in OUTPUTS:
        setattr(r, name.replace("g_", "o_", 1), refs[at])
        at += 1
    for name in CHANNELS:
        setattr(c, name, (refs[at], refs[at + 1]))
        at += 2
    in_sems, out_sems = refs[at], refs[at + 1]
    for i, name in enumerate(INPUTS):
        setattr(local, name[2:], in_sems.at[i])
    for i, name in enumerate(OUTPUTS):
        setattr(result, name[2:], out_sems.at[i])

    me, tx = lax.axis_index("sp"), lax.axis_index("tp")
    z, j = me // 8, me % 8
    partner = j + 1 - 2 * (j % 2)
    right, left, opp = (tx + 1) % 4, (tx + 3) % 4, (tx + 2) % 4
    column = pl.multiple_of(tx * 512, 512)

    barrier = pltpu.get_barrier_semaphore()

    @pl.loop(1, 64)
    def _(d):
        peer = (me + d) % 64
        pl.semaphore_signal(barrier, inc=1, device_id=(peer, tx), device_id_type=MESH)

    for side in (right, left):
        pl.semaphore_signal(barrier, inc=1, device_id=(me, side), device_id_type=MESH)

    loads = dict(
        routes=(r.h_routes, r.routes),
        route_weights=(r.h_route_weights, r.route_weights),
        cot=(r.h_cot.at[:, pl.ds(column, 512)], r.cot),
        rows=(r.h_rows, r.full.at[tx]),
        log_decay=(r.h_log_decay, r.log_decay),
        k=(r.h_k, r.k),
        v=(r.h_v, r.v),
        out_weight=(r.h_out_weight, r.out_weight),
        q=(r.h_q, r.q),
        w_gate=(r.h_w_gate, r.w_gate),
        w_up=(r.h_w_up, r.w_up),
        w_down=(r.h_w_down, r.w_down),
        gate=(r.h_gate, r.gate),
    )
    for name, (source, target) in loads.items():
        pltpu.make_async_copy(source, target, getattr(local, name)).start()

    def loaded(target, sem):
        pltpu.make_async_copy(target, target, sem).wait()

    def store(source, target, sem):
        pltpu.make_async_copy(source, target, sem).start()

    def send(src, dst, channel, n, sp, tp):
        out_sem, in_sem = channel
        pltpu.make_async_remote_copy(
            src_ref=src,
            dst_ref=dst,
            send_sem=out_sem.at[n],
            recv_sem=in_sem.at[n],
            device_id=(sp, tp),
            device_id_type=MESH,
        ).start()

    def got(ref, channel, n=0):
        pltpu.make_async_copy(ref, ref, channel[1].at[n]).wait()

    def sent(ref, channel, n=0):
        pltpu.make_async_copy(ref, ref, channel[0].at[n]).wait()

    class Ring:
        def __init__(self, piece, channel, members, targets):
            self.piece, self.channel = piece, channel
            self.mine, self.right, self.left, self.opp = members
            self.to_right, self.to_left = targets

        def go(self, n, h, sem, target):
            part = self.piece(n, h)
            send(part, part, self.channel, sem, *target)

        def start(self):
            self.go(self.mine, 0, 0, self.to_right)
            self.go(self.mine, 1, 2, self.to_left)
            self.go(self.mine, 1, 1, self.to_right)
            self.go(self.mine, 0, 3, self.to_left)

        def step(self):
            got(self.piece(self.left, 0), self.channel, 0)
            self.go(self.left, 0, 4, self.to_right)
            got(self.piece(self.right, 1), self.channel, 2)
            self.go(self.right, 1, 5, self.to_left)

        def near(self):
            got(self.piece(self.left, 1), self.channel, 1)
            got(self.piece(self.right, 0), self.channel, 3)

        def far(self):
            got(self.piece(self.opp, 0), self.channel, 4)
            got(self.piece(self.opp, 1), self.channel, 5)

        def sent(self):
            for sem, n, h in ((0, self.mine, 0), (1, self.mine, 1), (2, self.mine, 1), (3, self.mine, 0)):
                sent(self.piece(n, h), self.channel, sem)
            sent(self.piece(self.left, 0), self.channel, 4)
            sent(self.piece(self.right, 1), self.channel, 5)

    def tp_ring(buf, channel):
        half = buf.shape[1] // 2
        piece = lambda n, h: buf.at[n, pl.ds(h * half, half)]
        return Ring(piece, channel, (tx, right, left, opp), ((me, right), (me, left)))

    def y_ring(piece, channel):
        members = (j, (j + 2) % 8, (j + 6) % 8, (j + 4) % 8)
        return Ring(piece, channel, members, ((z * 8 + members[1], tx), (z * 8 + members[2], tx)))

    rows_ring = tp_ring(r.full, c.rows)
    arrived_ring = tp_ring(r.arr, c.arrived)
    residual_ring = tp_ring(r.resid, c.residual)
    weight_ring = y_ring(lambda n, h: r.weight.at[pl.ds(4 * h, 4), n], c.weight_y)
    mixed_ring = y_ring(lambda n, h: r.mixed.at[n, pl.ds(64 * h, 64)], c.mixed_y)

    def share(ring, channel, *members):
        for n in members:
            for h in range(2):
                part = ring.piece(n, h)
                send(part, part, channel, 0, z * 8 + partner, tx)

    def to_all(out, into, channel):
        @pl.loop(1, 64)
        def _(d):
            peer = (me + d) % 64
            send(out.at[peer], into.at[me], channel, 0, peer, tx)

        into[me] = out[me]

    def to_group(out, into, channel):
        @pl.loop(1, 8)
        def _(d):
            peer = (j + d) % 8
            send(out.at[peer], into.at[j], channel, 0, z * 8 + peer, tx)

        into[j] = out[j]

    def to_planes(src, into, channel):
        @pl.loop(1, 8)
        def _(d):
            send(src, into.at[z], channel, 0, ((z + d) % 8) * 8 + j, tx)

    eye = hot(iota((128, 128), 0) == iota((128, 128), 1), F32)
    loaded(r.routes, local.routes)
    loaded(r.route_weights, local.route_weights)
    routes = dot(eye, r.routes[...].astype(F32), 1, 1, precision=HIGHEST)
    route_weights = dot(eye, r.route_weights[...], 1, 1, precision=HIGHEST)
    expert = iota((128, 64), 1).astype(F32)
    route = [routes[:, 0:1], routes[:, 1:2]]
    named = [hot(route[n] == expert, F32) for n in range(2)]
    strict = iota((128, 128), 0) > iota((128, 128), 1)
    earlier = dot(hot(strict), (named[0] + named[1]).astype(BF16))
    slot = iota((128, 512), 1).astype(F32)
    loaded(r.cot, local.cot)
    cot = r.cot[...].astype(F32)
    scaled = []
    for n in range(2):
        rank = jnp.sum(named[n] * earlier, axis=1, keepdims=True)
        upper = jnp.where(rank >= 3.0, 1.0, 0.0)
        base = route[n] * 8.0
        r.hit_a[n] = hot(slot == base + rank)
        for m in range(3):
            place = jnp.where(rank - 3.0 * upper == float(m), base + 6.0 + upper, -1.0)
            r.hit_b[n, m] = hot(slot == place)
        scaled.append((route_weights[:, n : n + 1] * cot).astype(BF16))
    for m in range(3):
        lanes = slice(m * 128, (m + 1) * 128)
        total = dot(r.hit_a[0], scaled[0][:, lanes], 0, 0)
        total = total + dot(r.hit_a[1], scaled[1][:, lanes], 0, 0)
        total = total + dot(r.hit_b[0, m], scaled[0][:, 384:512], 0, 0)
        total = total + dot(r.hit_b[1, m], scaled[1][:, 384:512], 0, 0)
        r.pack_out[:, :, lanes] = total.reshape(64, 8, 128).astype(BF16)
    pl.semaphore_wait(barrier, 65)
    to_all(r.pack_out, r.pack_in, c.dispatch)
    loaded(r.full.at[tx], local.rows)
    rows_ring.start()

    loaded(r.out_weight, local.out_weight)

    @pl.loop(1, 8)
    def _(d):
        send(r.out_weight, r.weight.at[z, j], c.weight_z, 0, ((z + d) % 8) * 8 + j, tx)

    r.weight[z, j] = r.out_weight[...]

    row, col = iota((128, 128), 0), iota((128, 128), 1)
    tri = hot(row >= col, F32)
    head_of = iota((16, 1024), 1) // 64 == iota((16, 1024), 0)
    loaded(r.log_decay, local.log_decay)
    loaded(r.v, local.v)
    loaded(r.k, local.k)
    log_decay = r.log_decay[...]
    cumulative = dot(tri, log_decay, 1, 1, precision=HIGHEST)
    r.c_col[...] = dot(cumulative, hot(iota((16, 128), 0) == iota((16, 128), 1), F32), precision=HIGHEST)
    r.c_row[...] = dot(log_decay, tri, 1, 1, precision=HIGHEST)
    r.c_exp[...] = dot(cumulative, hot(head_of, F32), precision=HIGHEST)
    c_exp = r.c_exp[...]
    r.from_start[...] = jnp.exp(c_exp)
    r.to_end[...] = jnp.exp(r.c_exp[127:128, :] - c_exp)
    r.v_end[0], r.v_end[1] = split(r.v[...].astype(F32) * r.to_end[...])
    for g in range(2):
        wide, k = slice(g * 512, (g + 1) * 512), r.k[:, g * 128 : (g + 1) * 128]
        own = dot(r.v_end[0, :, wide], k, 0, 0) + dot(r.v_end[1, :, wide], k, 0, 0)
        r.f_own[g * 4 : (g + 1) * 4] = own.reshape(4, 128, 128)
    total = dot(log_decay, jnp.ones((128, 128), F32), precision=HIGHEST)
    spread = hot(iota((64, 16), 0) // 4 == iota((64, 16), 1), F32)
    r.log_out[...] = dot(spread, total, precision=HIGHEST).reshape(8, 8, 128)
    to_group(r.f_own, r.f_in, c.f_j)
    to_group(r.log_out, r.log_in, c.f_jlog)

    place, packed = iota((384, 512), 0), iota((384, 512), 1)
    source, rank = place // 6, place % 6
    r.sel_a[...] = hot(packed == source * 8 + rank)
    for m in range(3):
        r.sel_b[m] = hot((packed == source * 8 + 6 + rank // 3) & (rank % 3 == m))

    lower = row >= col
    first = col < 64
    loaded(r.q, local.q)
    for g in range(2):
        r.qk[g] = dot(r.q[:, g * 128 : (g + 1) * 128], r.k[:, g * 128 : (g + 1) * 128], 1, 1)

    def masked_values(p):
        vp = r.v[:, pl.ds(pl.multiple_of(p * 128, 128), 128)].astype(F32)
        return jnp.concatenate(
            [jnp.where(first, vp, 0.0).astype(BF16), jnp.where(first, 0.0, vp).astype(BF16)], axis=0
        )

    @pl.loop(0, 8)
    def _(p):
        off = pl.multiple_of(p * 128, 128)
        qk = r.qk[p // 4]
        c_pair = r.c_exp[:, pl.ds(off, 128)]
        for n in range(2):
            down = jnp.minimum(c_pair[:, 64 * n : 64 * n + 1] - r.c_row[pl.ds(2 * p + n, 1), :], 0.0)
            decay = jnp.where(lower, jnp.exp(down), 0.0)
            r.decay[p, :, n * 128 : (n + 1) * 128] = decay
            lanes = slice(n * 128, (n + 1) * 128)
            r.score[0, p, :, lanes], r.score[1, p, :, lanes] = split(qk * decay)
        values = masked_values(p)
        r.y[:, pl.ds(off, 128)] = dot(r.score[0, p], values) + dot(r.score[1, p], values)

    rows_ring.step()

    def factor(log):
        e = jnp.exp(log)
        return jnp.concatenate(
            [jnp.broadcast_to(e[0:1], (64, 128)), jnp.broadcast_to(e[4:5], (64, 128))], axis=0
        )

    def carry_group(states, run_ref, reverse):
        run, log = jnp.zeros((128, 128), F32), jnp.zeros((8, 128), F32)
        for i in reversed(range(8)) if reverse else range(8):
            r.before[i] = run
            r.log_before[i] = log
            run = factor(r.log_in[i]) * run + states[i].astype(F32)
            log = log + r.log_in[i]
        run_ref[...] = run.astype(run_ref.dtype)
        return log

    def carry_planes(planes, back, reverse):
        run = jnp.zeros((128, 128), F32)
        for i in reversed(range(8)) if reverse else range(8):
            passed = i > z if reverse else i < z
            run = jnp.where(passed, factor(r.log_z[i]) * run + planes[i].astype(F32), run)
        for i in range(8):
            back[i] = r.before[i] + factor(r.log_before[i]) * run

    got(r.f_in.at[pl.ds(0, 7)], c.f_j)
    got(r.log_in.at[pl.ds(0, 7)], c.f_jlog)
    r.log_run[...] = carry_group(r.f_in, r.f_run, False)
    r.log_z[z] = r.log_run[...]
    r.f_z[z] = r.f_run[...]
    to_planes(r.f_run, r.f_z, c.f_z)
    to_planes(r.log_run, r.log_z, c.f_zlog)

    got(r.pack_in.at[pl.ds(0, 63)], c.dispatch)
    packed_in = r.pack_in[...].reshape(512, 384)
    r.arr[tx, :, 0:384] = dot(r.sel_a[...], packed_in).astype(BF16)
    tail = dot(r.sel_b[0], packed_in[:, 0:128])
    tail = tail + dot(r.sel_b[1], packed_in[:, 128:256])
    tail = tail + dot(r.sel_b[2], packed_in[:, 256:384])
    r.arr[tx, :, 384:512] = tail.astype(BF16)
    arrived_ring.start()

    rows_ring.near()
    rows_ring.far()
    loaded(r.w_gate, local.w_gate)
    loaded(r.w_up, local.w_up)
    loaded(r.w_down, local.w_down)
    gate_pre, up_pre = jnp.zeros((384, 256), F32), jnp.zeros((384, 256), F32)
    for t in range(4):
        gate_pre = gate_pre + dot(r.full[t], r.w_gate[t * 512 : (t + 1) * 512, :])
    r.gate_pre[...] = gate_pre
    for t in range(4):
        up_pre = up_pre + dot(r.full[t], r.w_up[t * 512 : (t + 1) * 512, :])
    r.up_pre[...] = up_pre
    gate_pre = r.gate_pre[...]
    r.hidden[...] = (gate_pre * sigmoid(gate_pre) * up_pre).astype(BF16)

    def hidden_part(t):
        return dot(r.arr[t], r.w_down[:, pl.ds(pl.multiple_of(t * 512, 512), 512)], 1, 1)

    r.hidden_grad[...] = hidden_part(tx)
    arrived_ring.step()
    arrived_ring.near()
    r.hidden_grad[...] += hidden_part(left)
    r.hidden_grad[...] += hidden_part(right)

    arrived_ring.far()
    hidden_grad = r.hidden_grad[...] + hidden_part(opp)
    gate_pre = r.gate_pre[...]
    gate_sig = sigmoid(gate_pre)
    slope = gate_sig * (1.0 + gate_pre * (1.0 - gate_sig))
    r.gate_grad[...] = (hidden_grad * r.up_pre[...] * slope).astype(BF16)
    r.up_grad[...] = (hidden_grad * (gate_pre * gate_sig)).astype(BF16)

    def row_part(t):
        rows = pl.ds(pl.multiple_of(t * 512, 512), 512)
        part = dot(r.gate_grad[...], r.w_gate[rows, :], 1, 1)
        return part + dot(r.up_grad[...], r.w_up[rows, :], 1, 1)

    top, bottom = pl.ds(0, 192), pl.ds(192, 192)
    r.rs_opp[...] = row_part(opp).astype(BF16)
    send(r.rs_opp.at[top], r.rs_half_l, c.scatter, 0, me, right)
    send(r.rs_opp.at[bottom], r.rs_half_r, c.scatter, 1, me, left)
    r.rs_own[...] = row_part(right)
    r.rs_right[bottom] = r.rs_own[bottom].astype(BF16)
    send(r.rs_right.at[bottom], r.rs_in_l.at[bottom], c.scatter, 2, me, right)
    r.rs_own_l[...] = row_part(left)
    r.rs_left[top] = r.rs_own_l[top].astype(BF16)
    send(r.rs_left.at[top], r.rs_in_r.at[top], c.scatter, 3, me, left)

    got(r.weight.at[pl.ds(0, 7), 0], c.weight_z)
    weight_ring.start()
    share(weight_ring, c.weight_c, j)

    got(r.rs_half_l, c.scatter, 0)
    r.rs_right[top] = (r.rs_own[top] + r.rs_half_l[...].astype(F32)).astype(BF16)
    send(r.rs_right.at[top], r.rs_in_l.at[top], c.scatter, 4, me, right)
    got(r.rs_half_r, c.scatter, 1)
    r.rs_left[bottom] = (r.rs_own_l[bottom] + r.rs_half_r[...].astype(F32)).astype(BF16)
    send(r.rs_left.at[bottom], r.rs_in_r.at[bottom], c.scatter, 5, me, left)
    r.rs_own[...] = row_part(tx)

    got(r.f_z.at[pl.ds(0, 7)], c.f_z)
    got(r.log_z.at[pl.ds(0, 7)], c.f_zlog)
    carry_planes(r.f_z, r.f_back, False)
    to_group(r.f_back, r.state, c.f_back)

    @pl.loop(0, 4)
    def _(t):
        rows = pl.ds(pl.multiple_of(t * 512, 512), 512)
        r.o_gate[rows, :] = dot(r.full[t], r.gate_grad[...], 0, 0).astype(BF16)
        r.o_up[rows, :] = dot(r.full[t], r.up_grad[...], 0, 0).astype(BF16)
        r.o_down[:, rows] = dot(r.hidden[...], r.arr[t], 0, 0).astype(BF16)

    store(r.o_gate, r.g_gate, result.gate)
    store(r.o_up, r.g_up, result.up)
    store(r.o_down, r.g_down, result.down)
    weight_ring.step()

    got(r.rs_in_l.at[bottom], c.scatter, 2)
    got(r.rs_in_l.at[top], c.scatter, 4)
    got(r.rs_in_r.at[top], c.scatter, 3)
    got(r.rs_in_r.at[bottom], c.scatter, 5)
    summed = r.rs_own[...] + r.rs_in_l[...].astype(F32) + r.rs_in_r[...].astype(F32)
    summed = summed.astype(BF16)
    for m in range(3):
        lanes = slice(m * 128, (m + 1) * 128)
        total = dot(r.sel_a[...], summed[:, lanes], 0, 0)
        total = total + dot(r.sel_b[m], summed[:, 384:512], 0, 0)
        r.ret_out[:, :, lanes] = total.reshape(64, 8, 128).astype(BF16)
    to_all(r.ret_out, r.ret_in, c.back)

    got(r.state.at[pl.ds(0, 7)], c.f_back)
    for g in range(2):
        lanes = slice(g * 512, (g + 1) * 512)
        high, low = split(r.state[g * 4 : (g + 1) * 4].reshape(512, 128))
        q = r.q[:, g * 128 : (g + 1) * 128]
        r.carried[:, lanes] = (dot(q, high, 1, 1) + dot(q, low, 1, 1)) * r.from_start[:, lanes]
    y = r.y[...] + r.carried[...]
    r.y[...] = y
    loaded(r.gate, local.gate)
    gate = r.gate[...].astype(F32)
    r.mixed[j] = (y * (gate * sigmoid(gate))).astype(BF16)
    mixed_ring.start()
    share(mixed_ring, c.mixed_c, j)
    weight_ring.near()
    weight_ring.far()
    share(weight_ring, c.weight_c, weight_ring.left, weight_ring.right, weight_ring.opp)
    mixed_ring.step()

    got(r.ret_in.at[pl.ds(0, 63)], c.back)
    packed_back = r.ret_in[...].reshape(512, 384)
    picked = dot(r.hit_a[0] + r.hit_a[1], packed_back)
    tail = dot(r.hit_b[0, 0] + r.hit_b[1, 0], packed_back[:, 0:128])
    tail = tail + dot(r.hit_b[0, 1] + r.hit_b[1, 1], packed_back[:, 128:256])
    tail = tail + dot(r.hit_b[0, 2] + r.hit_b[1, 2], packed_back[:, 256:384])
    picked = jnp.concatenate([picked, tail], axis=1)
    residual = r.cot[...].astype(F32) + picked
    r.resid[tx] = residual.astype(BF16)
    residual_ring.start()
    r.o_res[...] = residual
    store(r.o_res, r.g_res, result.res)
    residual_ring.step()
    got(r.weight.at[:, pl.ds(0, 4)], c.weight_c)
    residual_ring.near()
    residual_ring.far()

    @pl.loop(0, 4)
    def _(n):
        lanes = pl.ds(pl.multiple_of(n * 256, 256), 256)
        grad = jnp.zeros((128, 256), F32)
        for t in range(4):
            w = r.weight[2 * t : 2 * t + 2, :, :, lanes].reshape(512, 256)
            grad = grad + dot(r.resid[t], w)
        gate = r.gate[:, lanes].astype(F32)
        sig = sigmoid(gate)
        r.o_gate_in[:, lanes] = grad * r.y[:, lanes] * (sig * (1.0 + gate * (1.0 - sig)))
        dy = grad * (gate * sig)
        r.dy[:, lanes] = dy
        r.dy_start[0, :, lanes], r.dy_start[1, :, lanes] = split(dy * r.from_start[:, lanes])

    store(r.o_gate_in, r.g_gate_in, result.gate_in)
    for g in range(2):
        wide, q = slice(g * 512, (g + 1) * 512), r.q[:, g * 128 : (g + 1) * 128]
        reached = dot(r.dy_start[0, :, wide], q, 0, 0) + dot(r.dy_start[1, :, wide], q, 0, 0)
        r.b_own[g * 4 : (g + 1) * 4] = reached.reshape(4, 128, 128)
    to_group(r.b_own, r.b_in, c.b_j)

    for t in range(4):
        turned = dot(r.resid[t], eye.astype(BF16), 0, 0)
        r.res_t[2 * t : 2 * t + 2] = turned.reshape(2, 8, 32, 128).astype(BF16)

    @pl.loop(1, 8)
    def _(d):
        peer = (j + d) % 8
        send(r.res_t.at[:, peer], r.res_in.at[j], c.gow_j, 0, z * 8 + peer, tx)

    r.res_in[j] = r.res_t[:, j]

    mixed_ring.near()
    mixed_ring.far()
    share(mixed_ring, c.mixed_c, mixed_ring.left, mixed_ring.right, mixed_ring.opp)

    got(r.b_in.at[pl.ds(0, 7)], c.b_j)
    carry_group(r.b_in, r.b_run, True)
    r.b_z[z] = r.b_run[...]
    to_planes(r.b_run, r.b_z, c.b_z)

    got(r.res_in.at[pl.ds(0, 7)], c.gow_j)
    got(r.mixed.at[pl.ds(0, 4)], c.mixed_c)

    @pl.loop(0, 4)
    def _(n):
        lanes = pl.ds(pl.multiple_of(n * 256, 256), 256)
        part = jnp.zeros((256, 256), F32)
        for i in range(8):
            part = part + dot(r.res_in[i].reshape(256, 128), r.mixed[i, :, lanes])
        part = part.reshape(8, 32, 256)
        r.gow_part[:, :, lanes] = part
        r.gow_out[:, :, lanes] = part.astype(BF16)

    @pl.loop(1, 8)
    def _(d):
        plane = (z + d) % 8
        send(r.gow_out.at[plane], r.gow_in.at[z], c.gow_z, 0, plane * 8 + j, tx)

    r.row_col[...] = jnp.zeros((128, 128), F32)
    r.dqk[...] = jnp.zeros((2, 128, 128), F32)

    @pl.loop(0, 8)
    def _(p):
        off = pl.multiple_of(p * 128, 128)
        g = p // 4
        qk = r.qk[g]
        dy = r.dy[:, pl.ds(off, 128)]
        part = dot(dy.astype(BF16), masked_values(p), 1, 1) * r.decay[p]
        r.dqk[g] += part[:, 0:128] + part[:, 128:256]
        total = r.row_col[...]
        dv = jnp.zeros((128, 128), F32)
        for n in range(2):
            lanes = slice(n * 128, (n + 1) * 128)
            weighed = (part[:, lanes] * qk).astype(BF16)
            head = hot(col == 2 * p + n)
            total = total + dot(weighed, head) - dot(weighed, head, 0, 0)
            own = jnp.where(first, dy, 0.0) if n == 0 else jnp.where(first, 0.0, dy)
            dv = dv + dot(r.score[0, p, :, lanes], own.astype(BF16), 0, 0)
        r.row_col[...] = total
        r.dv[:, pl.ds(off, 128)] = dv

    by_head = hot(iota((1024, 128), 0) // 64 == iota((1024, 128), 1))
    r.row_col[...] += fine_dot(r.dy[...] * r.carried[...], by_head)
    for g in range(2):
        state = r.state[g * 4 : (g + 1) * 4].reshape(512, 128).astype(BF16)
        r.dq[:, g * 128 : (g + 1) * 128] = dot(r.dy_start[0, :, g * 512 : (g + 1) * 512], state)

    got(r.b_z.at[pl.ds(0, 7)], c.b_z)
    carry_planes(r.b_z, r.b_back, True)
    to_group(r.b_back, r.dstate, c.b_back)

    for g in range(2):
        lanes = slice(g * 128, (g + 1) * 128)
        r.o_q[:, lanes] = r.dq[:, lanes] + dot(r.dqk[g].astype(BF16), r.k[:, lanes])
    store(r.o_q, r.g_q, result.q)

    got(r.dstate.at[pl.ds(0, 7)], c.b_back)
    for g in range(2):
        lanes, wide = slice(g * 128, (g + 1) * 128), slice(g * 512, (g + 1) * 512)
        dstate, low = split(r.dstate[g * 4 : (g + 1) * 4].reshape(512, 128))
        k = r.k[:, lanes]
        through = (dot(k, dstate, 1, 1) + dot(k, low, 1, 1)) * r.to_end[:, wide]
        r.carried[:, wide] = through
        r.o_v[:, wide] = r.dv[:, wide] + through
        r.o_k[:, lanes] = dot(r.dqk[g].astype(BF16), r.q[:, lanes], 0, 0) + dot(r.v_end[0, :, wide], dstate)
    store(r.o_v, r.g_v, result.v)
    store(r.o_k, r.g_k, result.k)
    added = fine_dot(r.v[...].astype(F32) * r.carried[...], by_head)
    high, low = split((r.dstate[...] * r.state[...]).reshape(1024, 128))
    both = dot(by_head, high, 0, 0) + dot(by_head, low, 0, 0)
    kept = dot(jnp.ones((128, 128), F32), both, 1, 1, precision=HIGHEST)
    kept = kept * jnp.exp(r.c_col[127:128, :])
    upper = hot(row <= col, F32)
    below = hot(row > col, F32)
    grad = dot(upper, r.row_col[...], precision=HIGHEST) + dot(below, added, precision=HIGHEST) + kept
    r.o_decay[...] = dot(eye[0:16], grad, 1, 1, precision=HIGHEST)
    store(r.o_decay, r.g_decay, result.decay)

    got(r.gow_in.at[pl.ds(0, 7)], c.gow_z)
    total = r.gow_part[z]
    for d in range(1, 8):
        total = total + r.gow_in[(z + d) % 8].astype(F32)
    r.o_out[...] = total
    store(r.o_out, r.g_out, result.out)

    for ring in (rows_ring, arrived_ring, residual_ring, weight_ring, mixed_ring):
        ring.sent()
    sent(r.pack_out.at[pl.ds(0, 63)], c.dispatch)
    sent(r.ret_out.at[pl.ds(0, 63)], c.back)
    for n in range(6):
        sent(r.rs_half_l, c.scatter, n)
    sent(r.weight.at[pl.ds(0, 7), 0], c.weight_z)
    sent(r.weight.at[:, pl.ds(0, 4)], c.weight_c)
    sent(r.mixed.at[pl.ds(0, 4)], c.mixed_c)
    sent(r.res_in.at[pl.ds(0, 7)], c.gow_j)
    sent(r.gow_out.at[pl.ds(0, 7)], c.gow_z)
    for channel in (c.f_j, c.f_z, c.f_back, c.b_j, c.b_back):
        sent(r.f_in.at[pl.ds(0, 7)], channel)
    sent(r.b_z.at[pl.ds(0, 7)], c.b_z)
    for channel in (c.f_jlog, c.f_zlog):
        sent(r.log_in.at[pl.ds(0, 7)], channel)
    for name in OUTPUTS:
        target = getattr(r, name)
        loaded(target, getattr(result, name[2:]))


def shards(
    out_cotangent,
    routes,
    route_weights,
    expert_rows,
    w_gate,
    w_up,
    w_down,
    out_weight,
    values,
    keys,
    queries,
    log_decay,
    gate_input,
):
    arrays = [jax.ShapeDtypeStruct(shape, dtype) for shape, dtype in OUTPUTS.values()]
    held = [pltpu.VMEM(shape, dtype) for shape, dtype in OUTPUTS.values()]
    scratch = [pltpu.VMEM(shape, dtype) for shape, dtype in BUFFERS.values()] + held
    for n in CHANNELS.values():
        scratch += [pltpu.SemaphoreType.DMA((n,))] * 2
    scratch += [pltpu.SemaphoreType.DMA((len(INPUTS),)), pltpu.SemaphoreType.DMA((len(OUTPUTS),))]
    outs = pl.pallas_call(
        kernel,
        out_shape=arrays,
        in_specs=[pl.BlockSpec(memory_space=pl.ANY)] * len(INPUTS),
        out_specs=[pl.BlockSpec(memory_space=pl.ANY)] * len(OUTPUTS),
        scratch_shapes=scratch,
        compiler_params=pltpu.CompilerParams(
            has_side_effects=True, collective_id=0, vmem_limit_bytes=66_000_000
        ),
        name="layer_backward",
    )(
        out_cotangent,
        routes.T,
        route_weights.T,
        expert_rows[0],
        w_gate[0],
        w_up[0],
        w_down[0],
        out_weight,
        values,
        keys,
        queries,
        log_decay.T,
        gate_input,
    )
    outs = pl.pallas_call(
        publish,
        out_shape=arrays,
        in_specs=[pl.BlockSpec(memory_space=pl.ANY)] * len(OUTPUTS),
        out_specs=[pl.BlockSpec(memory_space=pl.ANY)] * len(OUTPUTS),
        scratch_shapes=held + [pltpu.SemaphoreType.DMA((2, len(OUTPUTS)))],
        compiler_params=pltpu.CompilerParams(vmem_limit_bytes=66_000_000),
        name="publish",
    )(*outs)
    outs = list(outs)
    outs[8] = outs[8].T
    return (outs[0][None], outs[1][None], outs[2][None]) + tuple(outs[3:])


def solution(mesh):
    sp, both = P("sp", None), P("sp", "tp")
    columns, hidden = P("sp", None, "tp"), P("sp", "tp", None)
    in_specs = (sp, sp, sp, columns, columns, columns, hidden) + (both,) * 6
    out_specs = (columns, columns, hidden) + (both,) * 7
    return jax.shard_map(
        shards, mesh=mesh, in_specs=in_specs, out_specs=out_specs, check_vma=False
    )
```

time: 574 us -> 121 us (0.21)
  waiting for transfers between devices: 343 us -> 0 us
  Pallas kernels: 0 us -> 120 us
  blocking collectives: 79.2 us -> 0 us
  local copies, waits for them, and re-layouts: 40.5 us -> 0 us
  matrix products: 39.5 us -> 0 us
  other arithmetic: 38.5 us -> 0 us
  between operations: 16.7 us -> 0.66 us
  starting transfers between devices: 11.2 us -> 0 us
    all_gather x9 -> x0, waiting for transfers between devices: 170 us -> none  [the longest x6 147 us: carried_in(): pieces = jax.tree.map(lambda part: lax.all_gather(part, axis), running)]
    reduce_scatter x2 -> x0, waiting for transfers between devices: 150 us -> none  [the longest x1 110 us: shards(): lax.psum_scatter(lax.dot_general(part_rows, mixed, (((0,), (0,)), ((), ()...]
    pallas_call x0 -> x2, Pallas kernels: none -> 120 us  [the longest x1 116 us: shards(): pl.pallas_call(kernel, out_shape=arrays, in_specs=[pl.BlockSpec(memory_sp...]
    all_gather x5 -> x0, blocking collectives: 48.5 us -> none  [the longest x4 38.2 us: carried_in(): pieces = jax.tree.map(lambda part: lax.all_gather(part, axis), running)]
    dot_general x22 -> x0, matrix products: 39.5 us -> none  [the longest x3 6.98 us: block_step(): within = jnp.einsum('tsgr,sgrp->tgrp', combined, grouped, precision=HIGHEST)]
    all_to_all x1 -> x0, blocking collectives: 30.6 us -> none  [shards(): lax.all_to_all(outgoing.reshape(experts_all, capacity, columns), SP, spli...]
    all_to_all x1 -> x0, waiting for transfers between devices: 21.1 us -> none  [shards(): lax.all_to_all(send_back, SP, split_axis=0, concat_axis=0, tiled=True)]
    add x6 -> x0, other arithmetic: 15.2 us -> none  [carry_combine(): later[0][:, None, None] * earlier[1] + later[1]]
  transfers between devices with their start and end apart: 12 -> 0, of which waited for: 9 -> 0; matrix products, arithmetic and copies ran while one was open for 13% -> 0% of each run, Pallas kernels for 0% -> 0%
where the time goes in v1:
time: 121 us
  Pallas kernels  120 us (99%)
    pallas_call x1, Pallas kernels, shards(): pl.pallas_call(kernel, out_shape=arrays, in_specs=[pl.BlockSpec(memory_sp...  116 us
    pallas_call x1, Pallas kernels, shards(): pl.pallas_call(publish, out_shape=arrays, in_specs=[pl.BlockSpec(memory_s...  3.87 us

profile of v1, /device:TPU:1, one launch (start us, length us, event | category | flops | bytes accessed | tf_op | source)
XLA Modules:
  0.0 120.7 jit_solution(13903868148352328245)
XLA Ops:
  0.6 116.2 %layer_backward.1 = (bf16[2048,256]{1,0:T(8,128)(2,1)}, bf16[2048,256]{1,0:T(8,128)(2,1)}, bf16[256,2048]{1,0:T(8,128)(2,1)}, f32[32,1024]{1,0:T(8,128)}, f32[12...) custom-call(bf16[128,2048]{1,0:T(8,128)(2,1)} %refs_0_.1, ...), custom_call_target="tpu_custom_call" | custom-call | tf_op jit(solution)/shard_map/layer_backward/pallas_call | solution.py:781
  116.9 3.9 %publish.1 = (bf16[2048,256]{1,0:T(8,128)(2,1)}, bf16[2048,256]{1,0:T(8,128)(2,1)}, bf16[256,2048]{1,0:T(8,128)(2,1)}, f32[32,1024]{1,0:T(8,128)}, f32[128,512]{...) custom-call(bf16[2048,256]{1,0:T(8,128)(2,1)} %get-tuple-element.30., ...), custom_call_target="tpu_custom_call" | custom-call | tf_op jit(solution)/shard_map/publish/pallas_call | solution.py:806

commit v2 on v1

--- a/solution.py
+++ b/solution.py
@@ -16,7 +16,6 @@
     w_gate=((2048, 256), BF16),
     w_up=((2048, 256), BF16),
     w_down=((256, 2048), BF16),
-    out_weight=((32, 1024), BF16),
     v=((128, 1024), BF16),
     k=((128, 256), BF16),
     q=((128, 256), BF16),
@@ -24,6 +23,7 @@
     gate=((128, 1024), BF16),
     pack_out=((64, 8, 384), BF16),
     pack_in=((64, 8, 384), BF16),
+    pack_sorted=((64, 8, 384), BF16),
     ret_out=((64, 8, 384), BF16),
     ret_in=((64, 8, 384), BF16),
     hit_a=((2, 128, 512), BF16),
@@ -41,15 +41,16 @@
     rs_opp=((384, 512), BF16),
     rs_right=((384, 512), BF16),
     rs_left=((384, 512), BF16),
-    rs_half_l=((192, 512), BF16),
-    rs_half_r=((192, 512), BF16),
+    rs_half_l=((384, 512), BF16),
+    rs_half_r=((384, 512), BF16),
     rs_in_l=((384, 512), BF16),
     rs_in_r=((384, 512), BF16),
     rs_own=((384, 512), F32),
     rs_own_l=((384, 512), F32),
+    rs_own_r=((384, 512), F32),
     resid=((4, 128, 512), BF16),
-    res_t=((8, 8, 32, 128), BF16),
-    res_in=((8, 8, 32, 128), BF16),
+    res_t=((2, 8, 32, 128), BF16),
+    res_in=((4, 8, 2, 32, 128), BF16),
     weight=((8, 8, 32, 1024), BF16),
     mixed=((8, 128, 1024), BF16),
     gow_part=((8, 32, 1024), F32),
@@ -67,7 +68,7 @@
     y=((128, 1024), F32),
     carried=((128, 1024), F32),
     dy=((128, 1024), F32),
-    dy_start=((2, 128, 1024), BF16),
+    dy_start=((128, 1024), BF16),
     dv=((128, 1024), F32),
     dqk=((2, 128, 128), F32),
     row_col=((128, 128), F32),
@@ -82,8 +83,8 @@
     f_in=((8, 128, 128), F32),
     f_run=((128, 128), F32),
     f_z=((8, 128, 128), F32),
-    f_back=((8, 128, 128), F32),
-    state=((8, 128, 128), F32),
+    f_back=((8, 128, 128), BF16),
+    state=((8, 128, 128), BF16),
     b_own=((8, 128, 128), F32),
     b_in=((8, 128, 128), F32),
     b_run=((128, 128), BF16),
@@ -98,12 +99,14 @@
     dispatch=1,
     back=1,
     scatter=6,
+    scatter_near=6,
     weight_z=1,
     weight_y=6,
     weight_c=1,
     mixed_y=6,
     mixed_c=1,
     gow_j=1,
+    columns=6,
     gow_z=1,
     f_j=1,
     f_jlog=1,
@@ -143,6 +146,10 @@
 )
 
 
+PLANES = (4, 3, 5, 2, 6, 1, 7, 0)
+FAR, NEAR = (0, 80, 144), (144, 256, 384)
+
+
 class Refs:
     pass
 
@@ -212,6 +219,7 @@
     partner = j + 1 - 2 * (j % 2)
     right, left, opp = (tx + 1) % 4, (tx + 3) % 4, (tx + 2) % 4
     column = pl.multiple_of(tx * 512, 512)
+    planes = [(z + d) % 8 for d in PLANES]
 
     barrier = pltpu.get_barrier_semaphore()
 
@@ -227,11 +235,10 @@
         routes=(r.h_routes, r.routes),
         route_weights=(r.h_route_weights, r.route_weights),
         cot=(r.h_cot.at[:, pl.ds(column, 512)], r.cot),
-        rows=(r.h_rows, r.full.at[tx]),
         log_decay=(r.h_log_decay, r.log_decay),
         k=(r.h_k, r.k),
         v=(r.h_v, r.v),
-        out_weight=(r.h_out_weight, r.out_weight),
+        out_weight=(r.h_out_weight, r.weight.at[z, j]),
         q=(r.h_q, r.q),
         w_gate=(r.h_w_gate, r.w_gate),
         w_up=(r.h_w_up, r.w_up),
@@ -240,6 +247,10 @@
     )
     for name, (source, target) in loads.items():
         pltpu.make_async_copy(source, target, getattr(local, name)).start()
+
+    for n in range(8):
+        source = r.h_rows.at[pl.ds(pl.multiple_of(planes[n] * 48, 16), 48)]
+        pltpu.make_async_copy(source, r.full.at[tx, pl.ds(n * 48, 48)], local.rows).start()
 
     def loaded(target, sem):
         pltpu.make_async_copy(target, target, sem).wait()
@@ -275,8 +286,14 @@
             send(part, part, self.channel, sem, *target)
 
         def start(self):
+            self.first()
+            self.second()
+
+        def first(self):
             self.go(self.mine, 0, 0, self.to_right)
             self.go(self.mine, 1, 2, self.to_left)
+
+        def second(self):
             self.go(self.mine, 1, 1, self.to_right)
             self.go(self.mine, 0, 3, self.to_left)
 
@@ -312,6 +329,8 @@
     rows_ring = tp_ring(r.full, c.rows)
     arrived_ring = tp_ring(r.arr, c.arrived)
     residual_ring = tp_ring(r.resid, c.residual)
+    columns_ring = tp_ring(r.res_in, c.columns)
+
     weight_ring = y_ring(lambda n, h: r.weight.at[pl.ds(4 * h, 4), n], c.weight_y)
     mixed_ring = y_ring(lambda n, h: r.mixed.at[n, pl.ds(64 * h, 64)], c.mixed_y)
 
@@ -321,13 +340,16 @@
                 part = ring.piece(n, h)
                 send(part, part, channel, 0, z * 8 + partner, tx)
 
-    def to_all(out, into, channel):
-        @pl.loop(1, 64)
+    def to_plane_members(out, into, channel, n, first):
+        own = PLANES[n] == 0
+
+        @pl.loop(1 if own else 0, 8)
         def _(d):
-            peer = (me + d) % 64
-            send(out.at[peer], into.at[me], channel, 0, peer, tx)
-
-        into[me] = out[me]
+            peer = (j + d) % 8
+            send(out.at[first + peer], into.at[me], channel, 0, planes[n] * 8 + peer, tx)
+
+        if own:
+            into[me] = out[first + j]
 
     def to_group(out, into, channel):
         @pl.loop(1, 8)
@@ -372,19 +394,6 @@
         total = total + dot(r.hit_b[0, m], scaled[0][:, 384:512], 0, 0)
         total = total + dot(r.hit_b[1, m], scaled[1][:, 384:512], 0, 0)
         r.pack_out[:, :, lanes] = total.reshape(64, 8, 128).astype(BF16)
-    pl.semaphore_wait(barrier, 65)
-    to_all(r.pack_out, r.pack_in, c.dispatch)
-    loaded(r.full.at[tx], local.rows)
-    rows_ring.start()
-
-    loaded(r.out_weight, local.out_weight)
-
-    @pl.loop(1, 8)
-    def _(d):
-        send(r.out_weight, r.weight.at[z, j], c.weight_z, 0, ((z + d) % 8) * 8 + j, tx)
-
-    r.weight[z, j] = r.out_weight[...]
-
     row, col = iota((128, 128), 0), iota((128, 128), 1)
     tri = hot(row >= col, F32)
     head_of = iota((16, 1024), 1) // 64 == iota((16, 1024), 0)
@@ -407,9 +416,6 @@
     total = dot(log_decay, jnp.ones((128, 128), F32), precision=HIGHEST)
     spread = hot(iota((64, 16), 0) // 4 == iota((64, 16), 1), F32)
     r.log_out[...] = dot(spread, total, precision=HIGHEST).reshape(8, 8, 128)
-    to_group(r.f_own, r.f_in, c.f_j)
-    to_group(r.log_out, r.log_in, c.f_jlog)
-
     place, packed = iota((384, 512), 0), iota((384, 512), 1)
     source, rank = place // 6, place % 6
     r.sel_a[...] = hot(packed == source * 8 + rank)
@@ -442,7 +448,16 @@
         values = masked_values(p)
         r.y[:, pl.ds(off, 128)] = dot(r.score[0, p], values) + dot(r.score[1, p], values)
 
+    pl.semaphore_wait(barrier, 65)
+    for n in range(8):
+        to_plane_members(r.pack_out, r.pack_in, c.dispatch, n, planes[n] * 8)
+    loaded(r.full.at[tx], local.rows)
+    rows_ring.start()
+    to_group(r.f_own, r.f_in, c.f_j)
+    to_group(r.log_out, r.log_in, c.f_jlog)
     rows_ring.step()
+    loaded(r.weight.at[z, j], local.out_weight)
+    to_planes(r.weight.at[z, j], r.weight.at[:, j], c.weight_z)
 
     def factor(log):
         e = jnp.exp(log)
@@ -466,7 +481,18 @@
             passed = i > z if reverse else i < z
             run = jnp.where(passed, factor(r.log_z[i]) * run + planes[i].astype(F32), run)
         for i in range(8):
-            back[i] = r.before[i] + factor(r.log_before[i]) * run
+            back[i] = (r.before[i] + factor(r.log_before[i]) * run).astype(back.dtype)
+
+    got(r.pack_in.at[pl.ds(0, 63)], c.dispatch)
+    for n in range(8):
+        r.pack_sorted[n * 8 : (n + 1) * 8] = r.pack_in[pl.ds(planes[n] * 8, 8)]
+    packed_in = r.pack_sorted[...].reshape(512, 384)
+    r.arr[tx, :, 0:384] = dot(r.sel_a[...], packed_in).astype(BF16)
+    tail = dot(r.sel_b[0], packed_in[:, 0:128])
+    tail = tail + dot(r.sel_b[1], packed_in[:, 128:256])
+    tail = tail + dot(r.sel_b[2], packed_in[:, 256:384])
+    r.arr[tx, :, 384:512] = tail.astype(BF16)
+    arrived_ring.start()
 
     got(r.f_in.at[pl.ds(0, 7)], c.f_j)
     got(r.log_in.at[pl.ds(0, 7)], c.f_jlog)
@@ -476,14 +502,6 @@
     to_planes(r.f_run, r.f_z, c.f_z)
     to_planes(r.log_run, r.log_z, c.f_zlog)
 
-    got(r.pack_in.at[pl.ds(0, 63)], c.dispatch)
-    packed_in = r.pack_in[...].reshape(512, 384)
-    r.arr[tx, :, 0:384] = dot(r.sel_a[...], packed_in).astype(BF16)
-    tail = dot(r.sel_b[0], packed_in[:, 0:128])
-    tail = tail + dot(r.sel_b[1], packed_in[:, 128:256])
-    tail = tail + dot(r.sel_b[2], packed_in[:, 256:384])
-    r.arr[tx, :, 384:512] = tail.astype(BF16)
-    arrived_ring.start()
 
     rows_ring.near()
     rows_ring.far()
@@ -509,6 +527,12 @@
     r.hidden_grad[...] += hidden_part(left)
     r.hidden_grad[...] += hidden_part(right)
 
+    got(r.weight.at[pl.ds(0, 7), 0], c.weight_z)
+    weight_ring.first()
+    share(weight_ring, c.weight_c, j)
+    weight_ring.second()
+
+
     arrived_ring.far()
     hidden_grad = r.hidden_grad[...] + hidden_part(opp)
     gate_pre = r.gate_pre[...]
@@ -517,38 +541,74 @@
     r.gate_grad[...] = (hidden_grad * r.up_pre[...] * slope).astype(BF16)
     r.up_grad[...] = (hidden_grad * (gate_pre * gate_sig)).astype(BF16)
 
-    def row_part(t):
+    def row_part(t, start, end):
         rows = pl.ds(pl.multiple_of(t * 512, 512), 512)
-        part = dot(r.gate_grad[...], r.w_gate[rows, :], 1, 1)
-        return part + dot(r.up_grad[...], r.w_up[rows, :], 1, 1)
-
-    top, bottom = pl.ds(0, 192), pl.ds(192, 192)
-    r.rs_opp[...] = row_part(opp).astype(BF16)
-    send(r.rs_opp.at[top], r.rs_half_l, c.scatter, 0, me, right)
-    send(r.rs_opp.at[bottom], r.rs_half_r, c.scatter, 1, me, left)
-    r.rs_own[...] = row_part(right)
-    r.rs_right[bottom] = r.rs_own[bottom].astype(BF16)
-    send(r.rs_right.at[bottom], r.rs_in_l.at[bottom], c.scatter, 2, me, right)
-    r.rs_own_l[...] = row_part(left)
-    r.rs_left[top] = r.rs_own_l[top].astype(BF16)
-    send(r.rs_left.at[top], r.rs_in_r.at[top], c.scatter, 3, me, left)
-
-    got(r.weight.at[pl.ds(0, 7), 0], c.weight_z)
-    weight_ring.start()
-    share(weight_ring, c.weight_c, j)
-
-    got(r.rs_half_l, c.scatter, 0)
-    r.rs_right[top] = (r.rs_own[top] + r.rs_half_l[...].astype(F32)).astype(BF16)
-    send(r.rs_right.at[top], r.rs_in_l.at[top], c.scatter, 4, me, right)
-    got(r.rs_half_r, c.scatter, 1)
-    r.rs_left[bottom] = (r.rs_own_l[bottom] + r.rs_half_r[...].astype(F32)).astype(BF16)
-    send(r.rs_left.at[bottom], r.rs_in_r.at[bottom], c.scatter, 5, me, left)
-    r.rs_own[...] = row_part(tx)
-
-    got(r.f_z.at[pl.ds(0, 7)], c.f_z)
-    got(r.log_z.at[pl.ds(0, 7)], c.f_zlog)
-    carry_planes(r.f_z, r.f_back, False)
-    to_group(r.f_back, r.state, c.f_back)
+        part = dot(r.gate_grad[start:end], r.w_gate[rows, :], 1, 1)
+        return part + dot(r.up_grad[start:end], r.w_up[rows, :], 1, 1)
+
+    def half_send(source, target, channel, n, start, end, side):
+        part = pl.ds(start, end - start)
+        send(source.at[part], target.at[part], channel, n, me, side)
+
+    def scatter_parts(group):
+        start, _, end = group
+        r.rs_opp[start:end] = row_part(opp, start, end).astype(BF16)
+        r.rs_own_r[start:end] = row_part(right, start, end)
+        r.rs_own_l[start:end] = row_part(left, start, end)
+
+    def scatter_start(group, channel):
+        start, middle, end = group
+        half_send(r.rs_opp, r.rs_half_l, channel, 0, start, middle, right)
+        half_send(r.rs_opp, r.rs_half_r, channel, 1, middle, end, left)
+        r.rs_right[middle:end] = r.rs_own_r[middle:end].astype(BF16)
+        half_send(r.rs_right, r.rs_in_l, channel, 2, middle, end, right)
+        r.rs_left[start:middle] = r.rs_own_l[start:middle].astype(BF16)
+        half_send(r.rs_left, r.rs_in_r, channel, 3, start, middle, left)
+
+    def scatter_step(group, channel):
+        start, middle, end = group
+        got(r.rs_half_l.at[pl.ds(start, middle - start)], channel, 0)
+        total = r.rs_own_r[start:middle] + r.rs_half_l[start:middle].astype(F32)
+        r.rs_right[start:middle] = total.astype(BF16)
+        half_send(r.rs_right, r.rs_in_l, channel, 4, start, middle, right)
+        got(r.rs_half_r.at[pl.ds(middle, end - middle)], channel, 1)
+        total = r.rs_own_l[middle:end] + r.rs_half_r[middle:end].astype(F32)
+        r.rs_left[middle:end] = total.astype(BF16)
+        half_send(r.rs_left, r.rs_in_r, channel, 5, middle, end, left)
+
+    def scatter_end(group, channel):
+        start, middle, end = group
+        top, bottom = pl.ds(start, middle - start), pl.ds(middle, end - middle)
+        got(r.rs_in_l.at[bottom], channel, 2)
+        got(r.rs_in_r.at[top], channel, 3)
+        got(r.rs_in_l.at[top], channel, 4)
+        got(r.rs_in_r.at[bottom], channel, 5)
+        total = r.rs_own[start:end] + r.rs_in_l[start:end].astype(F32)
+        return (total + r.rs_in_r[start:end].astype(F32)).astype(BF16)
+
+    def scatter_sent(group, channel):
+        start, middle, end = group
+        top, bottom = pl.ds(start, middle - start), pl.ds(middle, end - middle)
+        for n, part in enumerate((top, bottom, bottom, top, top, bottom)):
+            sent(r.rs_half_l.at[part], channel, n)
+
+    def pack_rows(summed, group, lanes, first, last):
+        start, _, end = group
+        skip = first * 8 - lanes.start
+        for m in range(3):
+            part = slice(m * 128, (m + 1) * 128)
+            total = dot(r.sel_a[start:end, lanes], summed[:, part], 0, 0)
+            total = total + dot(r.sel_b[m, start:end, lanes], summed[:, 384:512], 0, 0)
+            total = total[skip : skip + (last - first) * 8].reshape(last - first, 8, 128)
+            r.ret_out[first:last, :, part] = total.astype(BF16)
+
+    scatter_parts(FAR)
+    scatter_start(FAR, c.scatter)
+    scatter_parts(NEAR)
+    scatter_step(FAR, c.scatter)
+    scatter_start(NEAR, c.scatter_near)
+    weight_ring.step()
+    r.rs_own[...] = row_part(tx, 0, 384)
 
     @pl.loop(0, 4)
     def _(t):
@@ -560,38 +620,24 @@
     store(r.o_gate, r.g_gate, result.gate)
     store(r.o_up, r.g_up, result.up)
     store(r.o_down, r.g_down, result.down)
-    weight_ring.step()
-
-    got(r.rs_in_l.at[bottom], c.scatter, 2)
-    got(r.rs_in_l.at[top], c.scatter, 4)
-    got(r.rs_in_r.at[top], c.scatter, 3)
-    got(r.rs_in_r.at[bottom], c.scatter, 5)
-    summed = r.rs_own[...] + r.rs_in_l[...].astype(F32) + r.rs_in_r[...].astype(F32)
-    summed = summed.astype(BF16)
-    for m in range(3):
-        lanes = slice(m * 128, (m + 1) * 128)
-        total = dot(r.sel_a[...], summed[:, lanes], 0, 0)
-        total = total + dot(r.sel_b[m], summed[:, 384:512], 0, 0)
-        r.ret_out[:, :, lanes] = total.reshape(64, 8, 128).astype(BF16)
-    to_all(r.ret_out, r.ret_in, c.back)
-
-    got(r.state.at[pl.ds(0, 7)], c.f_back)
-    for g in range(2):
-        lanes = slice(g * 512, (g + 1) * 512)
-        high, low = split(r.state[g * 4 : (g + 1) * 4].reshape(512, 128))
-        q = r.q[:, g * 128 : (g + 1) * 128]
-        r.carried[:, lanes] = (dot(q, high, 1, 1) + dot(q, low, 1, 1)) * r.from_start[:, lanes]
-    y = r.y[...] + r.carried[...]
-    r.y[...] = y
-    loaded(r.gate, local.gate)
-    gate = r.gate[...].astype(F32)
-    r.mixed[j] = (y * (gate * sigmoid(gate))).astype(BF16)
-    mixed_ring.start()
-    share(mixed_ring, c.mixed_c, j)
+
+    summed = scatter_end(FAR, c.scatter)
+    pack_rows(summed, FAR, slice(0, 256), 0, 24)
+    for n in range(3):
+        to_plane_members(r.ret_out, r.ret_in, c.back, n, n * 8)
+    scatter_step(NEAR, c.scatter_near)
+
+    summed = scatter_end(NEAR, c.scatter_near)
+    pack_rows(summed, NEAR, slice(128, 512), 24, 64)
+    for n in range(3, 8):
+        to_plane_members(r.ret_out, r.ret_in, c.back, n, n * 8)
+    got(r.f_z.at[pl.ds(0, 7)], c.f_z)
+    got(r.log_z.at[pl.ds(0, 7)], c.f_zlog)
+    carry_planes(r.f_z, r.f_back, False)
+    to_group(r.f_back, r.state, c.f_back)
     weight_ring.near()
     weight_ring.far()
     share(weight_ring, c.weight_c, weight_ring.left, weight_ring.right, weight_ring.opp)
-    mixed_ring.step()
 
     got(r.ret_in.at[pl.ds(0, 63)], c.back)
     packed_back = r.ret_in[...].reshape(512, 384)
@@ -603,16 +649,42 @@
     residual = r.cot[...].astype(F32) + picked
     r.resid[tx] = residual.astype(BF16)
     residual_ring.start()
+
+    r.res_t[...] = dot(r.resid[tx], eye.astype(BF16), 0, 0).reshape(2, 8, 32, 128).astype(BF16)
+
+    @pl.loop(1, 8)
+    def _(d):
+        peer = (j + d) % 8
+        send(r.res_t.at[:, peer], r.res_in.at[tx, j], c.gow_j, 0, z * 8 + peer, tx)
+
+    r.res_in[tx, j] = r.res_t[:, j]
     r.o_res[...] = residual
     store(r.o_res, r.g_res, result.res)
+
+    got(r.state.at[pl.ds(0, 7)], c.f_back)
+    for g in range(2):
+        lanes = slice(g * 512, (g + 1) * 512)
+        state = r.state[g * 4 : (g + 1) * 4].reshape(512, 128)
+        r.carried[:, lanes] = dot(r.q[:, g * 128 : (g + 1) * 128], state, 1, 1) * r.from_start[:, lanes]
+    y = r.y[...] + r.carried[...]
+    r.y[...] = y
+    loaded(r.gate, local.gate)
+    gate = r.gate[...].astype(F32)
+    r.mixed[j] = (y * (gate * sigmoid(gate))).astype(BF16)
+    mixed_ring.start()
+    share(mixed_ring, c.mixed_c, j)
+
     residual_ring.step()
+    got(r.res_in.at[tx, pl.ds(0, 7)], c.gow_j)
+    columns_ring.start()
+
+    residual_ring.near()
+    mixed_ring.step()
+    residual_ring.far()
     got(r.weight.at[:, pl.ds(0, 4)], c.weight_c)
-    residual_ring.near()
-    residual_ring.far()
-
-    @pl.loop(0, 4)
-    def _(n):
-        lanes = pl.ds(pl.multiple_of(n * 256, 256), 256)
+
+    for n in range(4):
+        lanes = slice(n * 256, (n + 1) * 256)
         grad = jnp.zeros((128, 256), F32)
         for t in range(4):
             w = r.weight[2 * t : 2 * t + 2, :, :, lanes].reshape(512, 256)
@@ -622,36 +694,29 @@
         r.o_gate_in[:, lanes] = grad * r.y[:, lanes] * (sig * (1.0 + gate * (1.0 - sig)))
         dy = grad * (gate * sig)
         r.dy[:, lanes] = dy
-        r.dy_start[0, :, lanes], r.dy_start[1, :, lanes] = split(dy * r.from_start[:, lanes])
-
+        high, low = split(dy * r.from_start[:, lanes])
+        r.dy_start[:, lanes] = high
+        q = r.q[:, (n // 2) * 128 : (n // 2 + 1) * 128]
+        reached = dot(high, q, 0, 0) + dot(low, q, 0, 0)
+        r.b_own[2 * n : 2 * n + 2] = reached.reshape(2, 128, 128)
+        for peer in (2 * n, 2 * n + 1):
+
+            @pl.when(j != peer)
+            def _():
+                send(r.b_own.at[peer], r.b_in.at[j], c.b_j, 0, z * 8 + peer, tx)
+
+        if n == 1:
+            columns_ring.step()
+
+    r.b_in[j] = r.b_own[j]
     store(r.o_gate_in, r.g_gate_in, result.gate_in)
-    for g in range(2):
-        wide, q = slice(g * 512, (g + 1) * 512), r.q[:, g * 128 : (g + 1) * 128]
-        reached = dot(r.dy_start[0, :, wide], q, 0, 0) + dot(r.dy_start[1, :, wide], q, 0, 0)
-        r.b_own[g * 4 : (g + 1) * 4] = reached.reshape(4, 128, 128)
-    to_group(r.b_own, r.b_in, c.b_j)
-
-    for t in range(4):
-        turned = dot(r.resid[t], eye.astype(BF16), 0, 0)
-        r.res_t[2 * t : 2 * t + 2] = turned.reshape(2, 8, 32, 128).astype(BF16)
-
-    @pl.loop(1, 8)
-    def _(d):
-        peer = (j + d) % 8
-        send(r.res_t.at[:, peer], r.res_in.at[j], c.gow_j, 0, z * 8 + peer, tx)
-
-    r.res_in[j] = r.res_t[:, j]
 
     mixed_ring.near()
     mixed_ring.far()
     share(mixed_ring, c.mixed_c, mixed_ring.left, mixed_ring.right, mixed_ring.opp)
 
-    got(r.b_in.at[pl.ds(0, 7)], c.b_j)
-    carry_group(r.b_in, r.b_run, True)
-    r.b_z[z] = r.b_run[...]
-    to_planes(r.b_run, r.b_z, c.b_z)
-
-    got(r.res_in.at[pl.ds(0, 7)], c.gow_j)
+    columns_ring.near()
+    columns_ring.far()
     got(r.mixed.at[pl.ds(0, 4)], c.mixed_c)
 
     @pl.loop(0, 4)
@@ -659,15 +724,23 @@
         lanes = pl.ds(pl.multiple_of(n * 256, 256), 256)
         part = jnp.zeros((256, 256), F32)
         for i in range(8):
-            part = part + dot(r.res_in[i].reshape(256, 128), r.mixed[i, :, lanes])
+            part = part + dot(r.res_in[:, i].reshape(256, 128), r.mixed[i, :, lanes])
         part = part.reshape(8, 32, 256)
         r.gow_part[:, :, lanes] = part
         r.gow_out[:, :, lanes] = part.astype(BF16)
 
-    @pl.loop(1, 8)
-    def _(d):
-        plane = (z + d) % 8
-        send(r.gow_out.at[plane], r.gow_in.at[z], c.gow_z, 0, plane * 8 + j, tx)
+    def gow_send(*distances):
+        for d in distances:
+            plane = (z + d) % 8
+            send(r.gow_out.at[plane], r.gow_in.at[z], c.gow_z, 0, plane * 8 + j, tx)
+
+    gow_send(1, 7)
+
+    got(r.b_in.at[pl.ds(0, 7)], c.b_j)
+    carry_group(r.b_in, r.b_run, True)
+    r.b_z[z] = r.b_run[...]
+    to_planes(r.b_run, r.b_z, c.b_z)
+    gow_send(2, 6, 3, 5, 4)
 
     r.row_col[...] = jnp.zeros((128, 128), F32)
     r.dqk[...] = jnp.zeros((2, 128, 128), F32)
@@ -695,17 +768,18 @@
     by_head = hot(iota((1024, 128), 0) // 64 == iota((1024, 128), 1))
     r.row_col[...] += fine_dot(r.dy[...] * r.carried[...], by_head)
     for g in range(2):
-        state = r.state[g * 4 : (g + 1) * 4].reshape(512, 128).astype(BF16)
-        r.dq[:, g * 128 : (g + 1) * 128] = dot(r.dy_start[0, :, g * 512 : (g + 1) * 512], state)
-
-    got(r.b_z.at[pl.ds(0, 7)], c.b_z)
-    carry_planes(r.b_z, r.b_back, True)
-    to_group(r.b_back, r.dstate, c.b_back)
+        state = r.state[g * 4 : (g + 1) * 4].reshape(512, 128)
+        r.dq[:, g * 128 : (g + 1) * 128] = dot(r.dy_start[:, g * 512 : (g + 1) * 512], state)
 
     for g in range(2):
         lanes = slice(g * 128, (g + 1) * 128)
         r.o_q[:, lanes] = r.dq[:, lanes] + dot(r.dqk[g].astype(BF16), r.k[:, lanes])
     store(r.o_q, r.g_q, result.q)
+
+
+    got(r.b_z.at[pl.ds(0, 7)], c.b_z)
+    carry_planes(r.b_z, r.b_back, True)
+    to_group(r.b_back, r.dstate, c.b_back)
 
     got(r.dstate.at[pl.ds(0, 7)], c.b_back)
     for g in range(2):
@@ -719,7 +793,7 @@
     store(r.o_v, r.g_v, result.v)
     store(r.o_k, r.g_k, result.k)
     added = fine_dot(r.v[...].astype(F32) * r.carried[...], by_head)
-    high, low = split((r.dstate[...] * r.state[...]).reshape(1024, 128))
+    high, low = split((r.dstate[...] * r.state[...].astype(F32)).reshape(1024, 128))
     both = dot(by_head, high, 0, 0) + dot(by_head, low, 0, 0)
     kept = dot(jnp.ones((128, 128), F32), both, 1, 1, precision=HIGHEST)
     kept = kept * jnp.exp(r.c_col[127:128, :])
@@ -736,19 +810,20 @@
     r.o_out[...] = total
     store(r.o_out, r.g_out, result.out)
 
-    for ring in (rows_ring, arrived_ring, residual_ring, weight_ring, mixed_ring):
+    for ring in (rows_ring, arrived_ring, residual_ring, columns_ring, weight_ring, mixed_ring):
         ring.sent()
     sent(r.pack_out.at[pl.ds(0, 63)], c.dispatch)
     sent(r.ret_out.at[pl.ds(0, 63)], c.back)
-    for n in range(6):
-        sent(r.rs_half_l, c.scatter, n)
+    scatter_sent(FAR, c.scatter)
+    scatter_sent(NEAR, c.scatter_near)
     sent(r.weight.at[pl.ds(0, 7), 0], c.weight_z)
     sent(r.weight.at[:, pl.ds(0, 4)], c.weight_c)
     sent(r.mixed.at[pl.ds(0, 4)], c.mixed_c)
-    sent(r.res_in.at[pl.ds(0, 7)], c.gow_j)
+    sent(r.res_in.at[tx, pl.ds(0, 7)], c.gow_j)
     sent(r.gow_out.at[pl.ds(0, 7)], c.gow_z)
-    for channel in (c.f_j, c.f_z, c.f_back, c.b_j, c.b_back):
+    for channel in (c.f_j, c.f_z, c.b_j, c.b_back):
         sent(r.f_in.at[pl.ds(0, 7)], channel)
+    sent(r.state.at[pl.ds(0, 7)], c.f_back)
     sent(r.b_z.at[pl.ds(0, 7)], c.b_z)
     for channel in (c.f_jlog, c.f_zlog):
         sent(r.log_in.at[pl.ds(0, 7)], channel)

time: 121 us -> 112 us (0.926)
  Pallas kernels: 120 us -> 111 us
    pallas_call x1, Pallas kernels: 116 us -> 107 us  [shards(): pl.pallas_call(kernel, out_shape=arrays, in_specs=[pl.BlockSpec(memory_sp...]
where the time goes in v2:
time: 112 us
  Pallas kernels  111 us (99%)
    pallas_call x1, Pallas kernels, shards(): pl.pallas_call(kernel, out_shape=arrays, in_specs=[pl.BlockSpec(memory_sp...  107 us
    pallas_call x1, Pallas kernels, shards(): pl.pallas_call(publish, out_shape=arrays, in_specs=[pl.BlockSpec(memory_s...  3.87 us

profile of v2, /device:TPU:1, one launch (start us, length us, event | category | flops | bytes accessed | tf_op | source)
XLA Modules:
  0.0 111.8 jit_solution(4884609353958830484)
XLA Ops:
  0.6 107.3 %layer_backward.1 = (bf16[2048,256]{1,0:T(8,128)(2,1)}, bf16[2048,256]{1,0:T(8,128)(2,1)}, bf16[256,2048]{1,0:T(8,128)(2,1)}, f32[32,1024]{1,0:T(8,128)}, f32[12...) custom-call(bf16[128,2048]{1,0:T(8,128)(2,1)} %refs_0_.1, ...), custom_call_target="tpu_custom_call" | custom-call | tf_op jit(solution)/shard_map/layer_backward/pallas_call | solution.py:856
  108.0 3.9 %publish.1 = (bf16[2048,256]{1,0:T(8,128)(2,1)}, bf16[2048,256]{1,0:T(8,128)(2,1)}, bf16[256,2048]{1,0:T(8,128)(2,1)}, f32[32,1024]{1,0:T(8,128)}, f32[128,512]{...) custom-call(bf16[2048,256]{1,0:T(8,128)(2,1)} %get-tuple-element.30., ...), custom_call_target="tpu_custom_call" | custom-call | tf_op jit(solution)/shard_map/publish/pallas_call | solution.py:881

commit v3 on v2

--- a/solution.py
+++ b/solution.py
@@ -68,6 +68,7 @@
     y=((128, 1024), F32),
     carried=((128, 1024), F32),
     dy=((128, 1024), F32),
+    mixed_grad=((128, 1024), F32),
     dy_start=((128, 1024), BF16),
     dv=((128, 1024), F32),
     dqk=((2, 128, 128), F32),
@@ -87,16 +88,20 @@
     state=((8, 128, 128), BF16),
     b_own=((8, 128, 128), F32),
     b_in=((8, 128, 128), F32),
-    b_run=((128, 128), BF16),
-    b_z=((8, 128, 128), BF16),
+    b_run=((8, 16, 128), F32),
+    b_z=((8, 16, 128), F32),
+    b_scan=((8, 16, 128), F32),
+    b_pre=((8, 16, 128), F32),
     b_back=((8, 128, 128), F32),
     dstate=((8, 128, 128), F32),
 )
 CHANNELS = dict(
     rows=6,
     arrived=6,
-    residual=6,
+    arrived_near=6,
+    residual=3,
     dispatch=1,
+    dispatch_near=1,
     back=1,
     scatter=6,
     scatter_near=6,
@@ -106,7 +111,7 @@
     mixed_y=6,
     mixed_c=1,
     gow_j=1,
-    columns=6,
+    columns=3,
     gow_z=1,
     f_j=1,
     f_jlog=1,
@@ -115,6 +120,7 @@
     f_back=1,
     b_j=1,
     b_z=1,
+    b_pre=1,
     b_back=1,
 )
 INPUTS = dict(
@@ -184,35 +190,26 @@
 
 def publish(*refs):
     n = len(OUTPUTS)
-    sources, targets, held, sems = refs[:n], refs[n : 2 * n], refs[2 * n : 3 * n], refs[3 * n]
-    loads = [pltpu.make_async_copy(sources[i], held[i], sems.at[0, i]) for i in range(n)]
-    stores = [pltpu.make_async_copy(held[i], targets[i], sems.at[1, i]) for i in range(n)]
-    for load in loads:
-        load.start()
-    for load, store in zip(loads, stores):
-        load.wait()
+    sources, targets, sems = refs[:n], refs[n : 2 * n], refs[2 * n]
+    stores = [pltpu.make_async_copy(sources[i], targets[i], sems.at[i]) for i in range(n)]
+    for store in stores:
         store.start()
     for store in stores:
         store.wait()
 
 
 def kernel(*refs):
-    r, c, local, result = Refs(), Refs(), Refs(), Refs()
+    r, c, local = Refs(), Refs(), Refs()
     names = list(INPUTS) + list(OUTPUTS) + list(BUFFERS)
     for name, ref in zip(names, refs):
         setattr(r, name, ref)
     at = len(names)
-    for name in OUTPUTS:
-        setattr(r, name.replace("g_", "o_", 1), refs[at])
-        at += 1
     for name in CHANNELS:
         setattr(c, name, (refs[at], refs[at + 1]))
         at += 2
-    in_sems, out_sems = refs[at], refs[at + 1]
+    in_sems = refs[at]
     for i, name in enumerate(INPUTS):
         setattr(local, name[2:], in_sems.at[i])
-    for i, name in enumerate(OUTPUTS):
-        setattr(result, name[2:], out_sems.at[i])
 
     me, tx = lax.axis_index("sp"), lax.axis_index("tp")
     z, j = me // 8, me % 8
@@ -228,7 +225,7 @@
         peer = (me + d) % 64
         pl.semaphore_signal(barrier, inc=1, device_id=(peer, tx), device_id_type=MESH)
 
-    for side in (right, left):
+    for side in (right, left, opp):
         pl.semaphore_signal(barrier, inc=1, device_id=(me, side), device_id_type=MESH)
 
     loads = dict(
@@ -255,9 +252,6 @@
     def loaded(target, sem):
         pltpu.make_async_copy(target, target, sem).wait()
 
-    def store(source, target, sem):
-        pltpu.make_async_copy(source, target, sem).start()
-
     def send(src, dst, channel, n, sp, tp):
         out_sem, in_sem = channel
         pltpu.make_async_remote_copy(
@@ -317,19 +311,40 @@
             sent(self.piece(self.left, 0), self.channel, 4)
             sent(self.piece(self.right, 1), self.channel, 5)
 
-    def tp_ring(buf, channel):
-        half = buf.shape[1] // 2
-        piece = lambda n, h: buf.at[n, pl.ds(h * half, half)]
+    def tp_ring(buf, channel, group=None):
+        start, middle, end = group or (0, buf.shape[1] // 2, buf.shape[1])
+        parts = (pl.ds(start, middle - start), pl.ds(middle, end - middle))
+        piece = lambda n, h: buf.at[n, parts[h]]
         return Ring(piece, channel, (tx, right, left, opp), ((me, right), (me, left)))
+
+    class Direct:
+        def __init__(self, buf, channel):
+            self.buf, self.channel = buf, channel
+
+        def start(self):
+            for n, side in enumerate((right, left, opp)):
+                send(self.buf.at[tx], self.buf.at[tx], self.channel, n, me, side)
+
+        def near(self):
+            got(self.buf.at[left], self.channel, 0)
+            got(self.buf.at[right], self.channel, 1)
+
+        def far(self):
+            got(self.buf.at[opp], self.channel, 2)
+
+        def sent(self):
+            for n in range(3):
+                sent(self.buf.at[tx], self.channel, n)
 
     def y_ring(piece, channel):
         members = (j, (j + 2) % 8, (j + 6) % 8, (j + 4) % 8)
         return Ring(piece, channel, members, ((z * 8 + members[1], tx), (z * 8 + members[2], tx)))
 
     rows_ring = tp_ring(r.full, c.rows)
-    arrived_ring = tp_ring(r.arr, c.arrived)
-    residual_ring = tp_ring(r.resid, c.residual)
-    columns_ring = tp_ring(r.res_in, c.columns)
+    far_ring = tp_ring(r.arr, c.arrived, FAR)
+    near_ring = tp_ring(r.arr, c.arrived_near, NEAR)
+    residual_ring = Direct(r.resid, c.residual)
+    columns_ring = Direct(r.res_in, c.columns)
 
     weight_ring = y_ring(lambda n, h: r.weight.at[pl.ds(4 * h, 4), n], c.weight_y)
     mixed_ring = y_ring(lambda n, h: r.mixed.at[n, pl.ds(64 * h, 64)], c.mixed_y)
@@ -358,6 +373,14 @@
             send(out.at[peer], into.at[j], channel, 0, z * 8 + peer, tx)
 
         into[j] = out[j]
+
+    def across_planes(out, into, channel):
+        @pl.loop(1, 8)
+        def _(d):
+            plane = (z + d) % 8
+            send(out.at[plane], into.at[z], channel, 0, plane * 8 + j, tx)
+
+        into[z] = out[z]
 
     def to_planes(src, into, channel):
         @pl.loop(1, 8)
@@ -448,9 +471,10 @@
         values = masked_values(p)
         r.y[:, pl.ds(off, 128)] = dot(r.score[0, p], values) + dot(r.score[1, p], values)
 
-    pl.semaphore_wait(barrier, 65)
+    pl.semaphore_wait(barrier, 66)
     for n in range(8):
-        to_plane_members(r.pack_out, r.pack_in, c.dispatch, n, planes[n] * 8)
+        channel = c.dispatch if n < 3 else c.dispatch_near
+        to_plane_members(r.pack_out, r.pack_in, channel, n, planes[n] * 8)
     loaded(r.full.at[tx], local.rows)
     rows_ring.start()
     to_group(r.f_own, r.f_in, c.f_j)
@@ -472,27 +496,44 @@
             r.log_before[i] = log
             run = factor(r.log_in[i]) * run + states[i].astype(F32)
             log = log + r.log_in[i]
-        run_ref[...] = run.astype(run_ref.dtype)
+        run_ref[...] = run.reshape(run_ref.shape)
         return log
 
-    def carry_planes(planes, back, reverse):
+    def scan_planes(planes_in, scan):
+        run = jnp.zeros((16, 128), F32)
+        for i in reversed(range(8)):
+            scan[i] = run
+            run = jnp.exp(r.log_z[i, pl.ds(4 * (z // 4), 1), :]) * run + planes_in[i]
+
+    def carry_planes(planes, back):
         run = jnp.zeros((128, 128), F32)
-        for i in reversed(range(8)) if reverse else range(8):
-            passed = i > z if reverse else i < z
-            run = jnp.where(passed, factor(r.log_z[i]) * run + planes[i].astype(F32), run)
+        for i in range(8):
+            run = jnp.where(i < z, factor(r.log_z[i]) * run + planes[i], run)
+        back_to_group(run, back)
+
+    def back_to_group(run, back):
         for i in range(8):
             back[i] = (r.before[i] + factor(r.log_before[i]) * run).astype(back.dtype)
 
-    got(r.pack_in.at[pl.ds(0, 63)], c.dispatch)
-    for n in range(8):
-        r.pack_sorted[n * 8 : (n + 1) * 8] = r.pack_in[pl.ds(planes[n] * 8, 8)]
-    packed_in = r.pack_sorted[...].reshape(512, 384)
-    r.arr[tx, :, 0:384] = dot(r.sel_a[...], packed_in).astype(BF16)
-    tail = dot(r.sel_b[0], packed_in[:, 0:128])
-    tail = tail + dot(r.sel_b[1], packed_in[:, 128:256])
-    tail = tail + dot(r.sel_b[2], packed_in[:, 256:384])
-    r.arr[tx, :, 384:512] = tail.astype(BF16)
-    arrived_ring.start()
+    def unpack(group, lanes, first, last):
+        start, _, end = group
+        for n in range(first // 8, last // 8):
+            r.pack_sorted[n * 8 : (n + 1) * 8] = r.pack_in[pl.ds(planes[n] * 8, 8)]
+        packed = r.pack_sorted[lanes.start // 8 : lanes.stop // 8].reshape(lanes.stop - lanes.start, 384)
+        r.arr[tx, start:end, 0:384] = dot(r.sel_a[start:end, lanes], packed).astype(BF16)
+        tail = dot(r.sel_b[0, start:end, lanes], packed[:, 0:128])
+        tail = tail + dot(r.sel_b[1, start:end, lanes], packed[:, 128:256])
+        tail = tail + dot(r.sel_b[2, start:end, lanes], packed[:, 256:384])
+        r.arr[tx, start:end, 384:512] = tail.astype(BF16)
+
+    r.pack_sorted[24:32] = jnp.zeros((8, 8, 384), BF16)
+    got(r.pack_in.at[pl.ds(0, 24)], c.dispatch)
+    unpack(FAR, slice(0, 256), 0, 24)
+    far_ring.start()
+    got(r.pack_in.at[pl.ds(0, 39)], c.dispatch_near)
+    unpack(NEAR, slice(128, 512), 24, 64)
+    far_ring.step()
+    near_ring.start()
 
     got(r.f_in.at[pl.ds(0, 7)], c.f_j)
     got(r.log_in.at[pl.ds(0, 7)], c.f_jlog)
@@ -518,28 +559,18 @@
     gate_pre = r.gate_pre[...]
     r.hidden[...] = (gate_pre * sigmoid(gate_pre) * up_pre).astype(BF16)
 
-    def hidden_part(t):
-        return dot(r.arr[t], r.w_down[:, pl.ds(pl.multiple_of(t * 512, 512), 512)], 1, 1)
-
-    r.hidden_grad[...] = hidden_part(tx)
-    arrived_ring.step()
-    arrived_ring.near()
-    r.hidden_grad[...] += hidden_part(left)
-    r.hidden_grad[...] += hidden_part(right)
-
-    got(r.weight.at[pl.ds(0, 7), 0], c.weight_z)
-    weight_ring.first()
-    share(weight_ring, c.weight_c, j)
-    weight_ring.second()
-
-
-    arrived_ring.far()
-    hidden_grad = r.hidden_grad[...] + hidden_part(opp)
-    gate_pre = r.gate_pre[...]
-    gate_sig = sigmoid(gate_pre)
-    slope = gate_sig * (1.0 + gate_pre * (1.0 - gate_sig))
-    r.gate_grad[...] = (hidden_grad * r.up_pre[...] * slope).astype(BF16)
-    r.up_grad[...] = (hidden_grad * (gate_pre * gate_sig)).astype(BF16)
+    def hidden_part(t, group):
+        lanes = pl.ds(pl.multiple_of(t * 512, 512), 512)
+        return dot(r.arr[t, group[0] : group[2]], r.w_down[:, lanes], 1, 1)
+
+    def hidden_grads(group):
+        start, _, end = group
+        hidden_grad = r.hidden_grad[start:end] + hidden_part(opp, group)
+        gate_pre = r.gate_pre[start:end]
+        gate_sig = sigmoid(gate_pre)
+        slope = gate_sig * (1.0 + gate_pre * (1.0 - gate_sig))
+        r.gate_grad[start:end] = (hidden_grad * r.up_pre[start:end] * slope).astype(BF16)
+        r.up_grad[start:end] = (hidden_grad * (gate_pre * gate_sig)).astype(BF16)
 
     def row_part(t, start, end):
         rows = pl.ds(pl.multiple_of(t * 512, 512), 512)
@@ -602,43 +633,68 @@
             total = total[skip : skip + (last - first) * 8].reshape(last - first, 8, 128)
             r.ret_out[first:last, :, part] = total.astype(BF16)
 
+    r.hidden_grad[0:144] = hidden_part(tx, FAR)
+    far_ring.near()
+    r.hidden_grad[0:144] += hidden_part(left, FAR)
+    r.hidden_grad[0:144] += hidden_part(right, FAR)
+    far_ring.far()
+    hidden_grads(FAR)
     scatter_parts(FAR)
     scatter_start(FAR, c.scatter)
+    near_ring.step()
+    r.hidden_grad[144:384] = hidden_part(tx, NEAR)
+    scatter_step(FAR, c.scatter)
+
+    got(r.weight.at[pl.ds(0, 7), 0], c.weight_z)
+    weight_ring.first()
+    share(weight_ring, c.weight_c, j)
+    weight_ring.second()
+
+    near_ring.near()
+    r.hidden_grad[144:384] += hidden_part(left, NEAR)
+    r.hidden_grad[144:384] += hidden_part(right, NEAR)
+    near_ring.far()
+    hidden_grads(NEAR)
     scatter_parts(NEAR)
-    scatter_step(FAR, c.scatter)
     scatter_start(NEAR, c.scatter_near)
-    weight_ring.step()
     r.rs_own[...] = row_part(tx, 0, 384)
-
-    @pl.loop(0, 4)
-    def _(t):
-        rows = pl.ds(pl.multiple_of(t * 512, 512), 512)
-        r.o_gate[rows, :] = dot(r.full[t], r.gate_grad[...], 0, 0).astype(BF16)
-        r.o_up[rows, :] = dot(r.full[t], r.up_grad[...], 0, 0).astype(BF16)
-        r.o_down[:, rows] = dot(r.hidden[...], r.arr[t], 0, 0).astype(BF16)
-
-    store(r.o_gate, r.g_gate, result.gate)
-    store(r.o_up, r.g_up, result.up)
-    store(r.o_down, r.g_down, result.down)
-
     summed = scatter_end(FAR, c.scatter)
     pack_rows(summed, FAR, slice(0, 256), 0, 24)
     for n in range(3):
         to_plane_members(r.ret_out, r.ret_in, c.back, n, n * 8)
+
+    got(r.f_z.at[pl.ds(0, 7)], c.f_z)
+    got(r.log_z.at[pl.ds(0, 7)], c.f_zlog)
+    carry_planes(r.f_z, r.f_back)
+    to_group(r.f_back, r.state, c.f_back)
     scatter_step(NEAR, c.scatter_near)
+
+    @pl.loop(0, 4)
+    def _(t):
+        rows = pl.ds(pl.multiple_of(t * 512, 512), 512)
+        r.g_gate[rows, :] = dot(r.full[t], r.gate_grad[...], 0, 0).astype(BF16)
+        r.g_up[rows, :] = dot(r.full[t], r.up_grad[...], 0, 0).astype(BF16)
+        r.g_down[:, rows] = dot(r.hidden[...], r.arr[t], 0, 0).astype(BF16)
+
 
     summed = scatter_end(NEAR, c.scatter_near)
     pack_rows(summed, NEAR, slice(128, 512), 24, 64)
     for n in range(3, 8):
         to_plane_members(r.ret_out, r.ret_in, c.back, n, n * 8)
-    got(r.f_z.at[pl.ds(0, 7)], c.f_z)
-    got(r.log_z.at[pl.ds(0, 7)], c.f_zlog)
-    carry_planes(r.f_z, r.f_back, False)
-    to_group(r.f_back, r.state, c.f_back)
+    weight_ring.step()
     weight_ring.near()
-    weight_ring.far()
-    share(weight_ring, c.weight_c, weight_ring.left, weight_ring.right, weight_ring.opp)
-
+    share(weight_ring, c.weight_c, weight_ring.left, weight_ring.right)
+
+    got(r.state.at[pl.ds(0, 7)], c.f_back)
+    for g in range(2):
+        lanes = slice(g * 512, (g + 1) * 512)
+        state = r.state[g * 4 : (g + 1) * 4].reshape(512, 128)
+        r.carried[:, lanes] = dot(r.q[:, g * 128 : (g + 1) * 128], state, 1, 1) * r.from_start[:, lanes]
+    y = r.y[...] + r.carried[...]
+    r.y[...] = y
+    loaded(r.gate, local.gate)
+    gate = r.gate[...].astype(F32)
+    r.mixed[j] = (y * (gate * sigmoid(gate))).astype(BF16)
     got(r.ret_in.at[pl.ds(0, 63)], c.back)
     packed_back = r.ret_in[...].reshape(512, 384)
     picked = dot(r.hit_a[0] + r.hit_a[1], packed_back)
@@ -658,40 +714,35 @@
         send(r.res_t.at[:, peer], r.res_in.at[tx, j], c.gow_j, 0, z * 8 + peer, tx)
 
     r.res_in[tx, j] = r.res_t[:, j]
-    r.o_res[...] = residual
-    store(r.o_res, r.g_res, result.res)
-
-    got(r.state.at[pl.ds(0, 7)], c.f_back)
-    for g in range(2):
-        lanes = slice(g * 512, (g + 1) * 512)
-        state = r.state[g * 4 : (g + 1) * 4].reshape(512, 128)
-        r.carried[:, lanes] = dot(r.q[:, g * 128 : (g + 1) * 128], state, 1, 1) * r.from_start[:, lanes]
-    y = r.y[...] + r.carried[...]
-    r.y[...] = y
-    loaded(r.gate, local.gate)
-    gate = r.gate[...].astype(F32)
-    r.mixed[j] = (y * (gate * sigmoid(gate))).astype(BF16)
+    r.g_res[...] = residual
+
     mixed_ring.start()
     share(mixed_ring, c.mixed_c, j)
 
-    residual_ring.step()
+    weight_ring.far()
+    share(weight_ring, c.weight_c, weight_ring.opp)
+
+    got(r.weight.at[:, pl.ds(0, 4)], c.weight_c)
+
+    def mixed_grad_part(t, lanes):
+        w = r.weight[pl.ds(2 * t, 2), :, :, lanes].reshape(512, 256)
+        return dot(r.resid[t], w)
+
+    residual_ring.near()
+    for n in range(4):
+        lanes = slice(n * 256, (n + 1) * 256)
+        grad = mixed_grad_part(tx, lanes) + mixed_grad_part(left, lanes)
+        r.mixed_grad[:, lanes] = grad + mixed_grad_part(right, lanes)
     got(r.res_in.at[tx, pl.ds(0, 7)], c.gow_j)
     columns_ring.start()
-
-    residual_ring.near()
-    mixed_ring.step()
     residual_ring.far()
-    got(r.weight.at[:, pl.ds(0, 4)], c.weight_c)
 
     for n in range(4):
         lanes = slice(n * 256, (n + 1) * 256)
-        grad = jnp.zeros((128, 256), F32)
-        for t in range(4):
-            w = r.weight[2 * t : 2 * t + 2, :, :, lanes].reshape(512, 256)
-            grad = grad + dot(r.resid[t], w)
+        grad = r.mixed_grad[:, lanes] + mixed_grad_part(opp, lanes)
         gate = r.gate[:, lanes].astype(F32)
         sig = sigmoid(gate)
-        r.o_gate_in[:, lanes] = grad * r.y[:, lanes] * (sig * (1.0 + gate * (1.0 - sig)))
+        r.g_gate_in[:, lanes] = grad * r.y[:, lanes] * (sig * (1.0 + gate * (1.0 - sig)))
         dy = grad * (gate * sig)
         r.dy[:, lanes] = dy
         high, low = split(dy * r.from_start[:, lanes])
@@ -705,15 +756,21 @@
             def _():
                 send(r.b_own.at[peer], r.b_in.at[j], c.b_j, 0, z * 8 + peer, tx)
 
-        if n == 1:
-            columns_ring.step()
 
     r.b_in[j] = r.b_own[j]
-    store(r.o_gate_in, r.g_gate_in, result.gate_in)
-
+
+    mixed_ring.step()
+
+    got(r.b_in.at[pl.ds(0, 7)], c.b_j)
+    carry_group(r.b_in, r.b_run, True)
+    across_planes(r.b_run, r.b_z, c.b_z)
     mixed_ring.near()
     mixed_ring.far()
     share(mixed_ring, c.mixed_c, mixed_ring.left, mixed_ring.right, mixed_ring.opp)
+
+    got(r.b_z.at[pl.ds(0, 7)], c.b_z)
+    scan_planes(r.b_z, r.b_scan)
+    across_planes(r.b_scan, r.b_pre, c.b_pre)
 
     columns_ring.near()
     columns_ring.far()
@@ -736,11 +793,10 @@
 
     gow_send(1, 7)
 
-    got(r.b_in.at[pl.ds(0, 7)], c.b_j)
-    carry_group(r.b_in, r.b_run, True)
-    r.b_z[z] = r.b_run[...]
-    to_planes(r.b_run, r.b_z, c.b_z)
-    gow_send(2, 6, 3, 5, 4)
+    got(r.b_pre.at[pl.ds(0, 7)], c.b_pre)
+    back_to_group(r.b_pre[...].reshape(128, 128), r.b_back)
+    to_group(r.b_back, r.dstate, c.b_back)
+    gow_send(3, 5, 4, 2, 6)
 
     r.row_col[...] = jnp.zeros((128, 128), F32)
     r.dqk[...] = jnp.zeros((2, 128, 128), F32)
@@ -773,13 +829,8 @@
 
     for g in range(2):
         lanes = slice(g * 128, (g + 1) * 128)
-        r.o_q[:, lanes] = r.dq[:, lanes] + dot(r.dqk[g].astype(BF16), r.k[:, lanes])
-    store(r.o_q, r.g_q, result.q)
-
-
-    got(r.b_z.at[pl.ds(0, 7)], c.b_z)
-    carry_planes(r.b_z, r.b_back, True)
-    to_group(r.b_back, r.dstate, c.b_back)
+        r.g_q[:, lanes] = r.dq[:, lanes] + dot(r.dqk[g].astype(BF16), r.k[:, lanes])
+
 
     got(r.dstate.at[pl.ds(0, 7)], c.b_back)
     for g in range(2):
@@ -788,10 +839,8 @@
         k = r.k[:, lanes]
         through = (dot(k, dstate, 1, 1) + dot(k, low, 1, 1)) * r.to_end[:, wide]
         r.carried[:, wide] = through
-        r.o_v[:, wide] = r.dv[:, wide] + through
-        r.o_k[:, lanes] = dot(r.dqk[g].astype(BF16), r.q[:, lanes], 0, 0) + dot(r.v_end[0, :, wide], dstate)
-    store(r.o_v, r.g_v, result.v)
-    store(r.o_k, r.g_k, result.k)
+        r.g_v[:, wide] = r.dv[:, wide] + through
+        r.g_k[:, lanes] = dot(r.dqk[g].astype(BF16), r.q[:, lanes], 0, 0) + dot(r.v_end[0, :, wide], dstate)
     added = fine_dot(r.v[...].astype(F32) * r.carried[...], by_head)
     high, low = split((r.dstate[...] * r.state[...].astype(F32)).reshape(1024, 128))
     both = dot(by_head, high, 0, 0) + dot(by_head, low, 0, 0)
@@ -800,19 +849,18 @@
     upper = hot(row <= col, F32)
     below = hot(row > col, F32)
     grad = dot(upper, r.row_col[...], precision=HIGHEST) + dot(below, added, precision=HIGHEST) + kept
-    r.o_decay[...] = dot(eye[0:16], grad, 1, 1, precision=HIGHEST)
-    store(r.o_decay, r.g_decay, result.decay)
+    r.g_decay[...] = dot(eye[0:16], grad, 1, 1, precision=HIGHEST)
 
     got(r.gow_in.at[pl.ds(0, 7)], c.gow_z)
     total = r.gow_part[z]
     for d in range(1, 8):
         total = total + r.gow_in[(z + d) % 8].astype(F32)
-    r.o_out[...] = total
-    store(r.o_out, r.g_out, result.out)
-
-    for ring in (rows_ring, arrived_ring, residual_ring, columns_ring, weight_ring, mixed_ring):
+    r.g_out[...] = total
+
+    for ring in (rows_ring, far_ring, near_ring, residual_ring, columns_ring, weight_ring, mixed_ring):
         ring.sent()
-    sent(r.pack_out.at[pl.ds(0, 63)], c.dispatch)
+    sent(r.pack_out.at[pl.ds(0, 24)], c.dispatch)
+    sent(r.pack_out.at[pl.ds(0, 39)], c.dispatch_near)
     sent(r.ret_out.at[pl.ds(0, 63)], c.back)
     scatter_sent(FAR, c.scatter)
     scatter_sent(NEAR, c.scatter_near)
@@ -825,11 +873,9 @@
         sent(r.f_in.at[pl.ds(0, 7)], channel)
     sent(r.state.at[pl.ds(0, 7)], c.f_back)
     sent(r.b_z.at[pl.ds(0, 7)], c.b_z)
+    sent(r.b_z.at[pl.ds(0, 7)], c.b_pre)
     for channel in (c.f_jlog, c.f_zlog):
         sent(r.log_in.at[pl.ds(0, 7)], channel)
-    for name in OUTPUTS:
-        target = getattr(r, name)
-        loaded(target, getattr(result, name[2:]))
 
 
 def shards(
@@ -848,22 +894,11 @@
     gate_input,
 ):
     arrays = [jax.ShapeDtypeStruct(shape, dtype) for shape, dtype in OUTPUTS.values()]
-    held = [pltpu.VMEM(shape, dtype) for shape, dtype in OUTPUTS.values()]
-    scratch = [pltpu.VMEM(shape, dtype) for shape, dtype in BUFFERS.values()] + held
+    scratch = [pltpu.VMEM(shape, dtype) for shape, dtype in BUFFERS.values()]
     for n in CHANNELS.values():
         scratch += [pltpu.SemaphoreType.DMA((n,))] * 2
-    scratch += [pltpu.SemaphoreType.DMA((len(INPUTS),)), pltpu.SemaphoreType.DMA((len(OUTPUTS),))]
-    outs = pl.pallas_call(
-        kernel,
-        out_shape=arrays,
-        in_specs=[pl.BlockSpec(memory_space=pl.ANY)] * len(INPUTS),
-        out_specs=[pl.BlockSpec(memory_space=pl.ANY)] * len(OUTPUTS),
-        scratch_shapes=scratch,
-        compiler_params=pltpu.CompilerParams(
-            has_side_effects=True, collective_id=0, vmem_limit_bytes=66_000_000
-        ),
-        name="layer_backward",
-    )(
+    scratch += [pltpu.SemaphoreType.DMA((len(INPUTS),))]
+    arguments = (
         out_cotangent,
         routes.T,
         route_weights.T,
@@ -879,12 +914,23 @@
         gate_input,
     )
     outs = pl.pallas_call(
+        kernel,
+        out_shape=arrays,
+        in_specs=[pl.BlockSpec(memory_space=pltpu.HBM)] * len(INPUTS),
+        out_specs=[pl.BlockSpec(memory_space=pltpu.VMEM)] * len(OUTPUTS),
+        scratch_shapes=scratch,
+        compiler_params=pltpu.CompilerParams(
+            has_side_effects=True, collective_id=0, vmem_limit_bytes=50000000
+        ),
+        name="layer_backward",
+    )(*[pltpu.with_memory_space_constraint(value, pltpu.HBM) for value in arguments])
+    outs = pl.pallas_call(
         publish,
         out_shape=arrays,
-        in_specs=[pl.BlockSpec(memory_space=pl.ANY)] * len(OUTPUTS),
-        out_specs=[pl.BlockSpec(memory_space=pl.ANY)] * len(OUTPUTS),
-        scratch_shapes=held + [pltpu.SemaphoreType.DMA((2, len(OUTPUTS)))],
-        compiler_params=pltpu.CompilerParams(vmem_limit_bytes=66_000_000),
+        in_specs=[pl.BlockSpec(memory_space=pltpu.VMEM)] * len(OUTPUTS),
+        out_specs=[pl.BlockSpec(memory_space=pltpu.HBM)] * len(OUTPUTS),
+        scratch_shapes=[pltpu.SemaphoreType.DMA((len(OUTPUTS),))],
+        compiler_params=pltpu.CompilerParams(vmem_limit_bytes=8_000_000),
         name="publish",
     )(*outs)
     outs = list(outs)

time: 112 us -> 108 us (0.964)
  Pallas kernels: 111 us -> 107 us
    pallas_call x1, Pallas kernels: 107 us -> 104 us  [shards(): pl.pallas_call(kernel, out_shape=arrays, in_specs=[pl.BlockSpec(memory_sp...]
    pallas_call x1, Pallas kernels: 3.87 us -> 2.31 us  [shards(): pl.pallas_call(publish, out_shape=arrays, in_specs=[pl.BlockSpec(memory_s...]
where the time goes in v3:
time: 108 us; the launch traced here: 107 us
  Pallas kernels  107 us (99%)
    pallas_call x1, Pallas kernels, shards(): pl.pallas_call(kernel, out_shape=arrays, in_specs=[pl.BlockSpec(memory_sp...  104 us
    pallas_call x1, Pallas kernels, shards(): pl.pallas_call(publish, out_shape=arrays, in_specs=[pl.BlockSpec(memory_s...  2.31 us

profile of v3, /device:TPU:1, one launch (start us, length us, event | category | flops | bytes accessed | tf_op | source)
XLA Modules:
  0.0 107.4 jit_solution(4027148616320140942)
XLA Ops:
  0.6 104.4 %layer_backward.1 = (bf16[2048,256]{1,0:T(8,128)(2,1)S(1)}, bf16[2048,256]{1,0:T(8,128)(2,1)S(1)}, bf16[256,2048]{1,0:T(8,128)(2,1)S(1)}, f32[32,1024]{1,0:T(8,1...) custom-call(bf16[128,2048]{1,0:T(8,128)(2,1)} %refs_0_.1, ...), custom_call_target="tpu_custom_call" | custom-call | tf_op jit(solution)/shard_map/layer_backward/pallas_call | solution.py:916
  105.1 2.3 %publish.1 = (bf16[2048,256]{1,0:T(8,128)(2,1)}, bf16[2048,256]{1,0:T(8,128)(2,1)}, bf16[256,2048]{1,0:T(8,128)(2,1)}, f32[32,1024]{1,0:T(8,128)}, f32[128,512]{...) custom-call(bf16[2048,256]{1,0:T(8,128)(2,1)S(1)} %get-tuple-element, ...), custom_call_target="tpu_custom_call" | custom-call | tf_op jit(solution)/shard_map/publish/pallas_call | solution.py:927

commit v4 on v3

--- a/solution.py
+++ b/solution.py
@@ -92,8 +92,12 @@
     b_z=((8, 16, 128), F32),
     b_scan=((8, 16, 128), F32),
     b_pre=((8, 16, 128), F32),
-    b_back=((8, 128, 128), F32),
+    b_plane=((128, 128), BF16),
+    b_planes=((8, 128, 128), BF16),
+    b_group=((8, 128, 128), F32),
+    b_log=((8, 8, 128), F32),
     dstate=((8, 128, 128), F32),
+    carry=((8, 128, 128), F32),
 )
 CHANNELS = dict(
     rows=6,
@@ -122,6 +126,8 @@
     b_z=1,
     b_pre=1,
     b_back=1,
+    b_group=1,
+    b_log=1,
 )
 INPUTS = dict(
     h_cot=((128, 2048), BF16),
@@ -735,6 +741,7 @@
         r.mixed_grad[:, lanes] = grad + mixed_grad_part(right, lanes)
     got(r.res_in.at[tx, pl.ds(0, 7)], c.gow_j)
     columns_ring.start()
+    mixed_ring.step()
     residual_ring.far()
 
     for n in range(4):
@@ -759,18 +766,16 @@
 
     r.b_in[j] = r.b_own[j]
 
-    mixed_ring.step()
+    mixed_ring.near()
+    share(mixed_ring, c.mixed_c, mixed_ring.left, mixed_ring.right)
 
     got(r.b_in.at[pl.ds(0, 7)], c.b_j)
     carry_group(r.b_in, r.b_run, True)
     across_planes(r.b_run, r.b_z, c.b_z)
-    mixed_ring.near()
+    to_group(r.before, r.b_group, c.b_group)
+    to_group(r.log_before, r.b_log, c.b_log)
     mixed_ring.far()
-    share(mixed_ring, c.mixed_c, mixed_ring.left, mixed_ring.right, mixed_ring.opp)
-
-    got(r.b_z.at[pl.ds(0, 7)], c.b_z)
-    scan_planes(r.b_z, r.b_scan)
-    across_planes(r.b_scan, r.b_pre, c.b_pre)
+    share(mixed_ring, c.mixed_c, mixed_ring.opp)
 
     columns_ring.near()
     columns_ring.far()
@@ -791,12 +796,20 @@
             plane = (z + d) % 8
             send(r.gow_out.at[plane], r.gow_in.at[z], c.gow_z, 0, plane * 8 + j, tx)
 
-    gow_send(1, 7)
+
+    got(r.b_z.at[pl.ds(0, 7)], c.b_z)
+    scan_planes(r.b_z, r.b_scan)
+    across_planes(r.b_scan, r.b_pre, c.b_pre)
+    gow_send(3, 5, 4, 2, 6, 1, 7)
 
     got(r.b_pre.at[pl.ds(0, 7)], c.b_pre)
-    back_to_group(r.b_pre[...].reshape(128, 128), r.b_back)
-    to_group(r.b_back, r.dstate, c.b_back)
-    gow_send(3, 5, 4, 2, 6)
+    r.b_plane[...] = r.b_pre[...].reshape(128, 128).astype(BF16)
+
+    @pl.loop(1, 8)
+    def _(d):
+        send(r.b_plane, r.b_planes.at[j], c.b_back, 0, z * 8 + (j + d) % 8, tx)
+
+    r.b_planes[j] = r.b_plane[...]
 
     r.row_col[...] = jnp.zeros((128, 128), F32)
     r.dqk[...] = jnp.zeros((2, 128, 128), F32)
@@ -832,7 +845,13 @@
         r.g_q[:, lanes] = r.dq[:, lanes] + dot(r.dqk[g].astype(BF16), r.k[:, lanes])
 
 
-    got(r.dstate.at[pl.ds(0, 7)], c.b_back)
+    got(r.b_group.at[pl.ds(0, 7)], c.b_group)
+    got(r.b_log.at[pl.ds(0, 7)], c.b_log)
+    for i in range(8):
+        r.carry[i] = factor(r.b_log[i])
+    got(r.b_planes.at[pl.ds(0, 7)], c.b_back)
+    for i in range(8):
+        r.dstate[i] = r.b_group[i] + r.carry[i] * r.b_planes[i].astype(F32)
     for g in range(2):
         lanes, wide = slice(g * 128, (g + 1) * 128), slice(g * 512, (g + 1) * 512)
         dstate, low = split(r.dstate[g * 4 : (g + 1) * 4].reshape(512, 128))
@@ -869,12 +888,13 @@
     sent(r.mixed.at[pl.ds(0, 4)], c.mixed_c)
     sent(r.res_in.at[tx, pl.ds(0, 7)], c.gow_j)
     sent(r.gow_out.at[pl.ds(0, 7)], c.gow_z)
-    for channel in (c.f_j, c.f_z, c.b_j, c.b_back):
+    for channel in (c.f_j, c.f_z, c.b_j, c.b_group):
         sent(r.f_in.at[pl.ds(0, 7)], channel)
+    sent(r.b_planes.at[pl.ds(0, 7)], c.b_back)
     sent(r.state.at[pl.ds(0, 7)], c.f_back)
     sent(r.b_z.at[pl.ds(0, 7)], c.b_z)
     sent(r.b_z.at[pl.ds(0, 7)], c.b_pre)
-    for channel in (c.f_jlog, c.f_zlog):
+    for channel in (c.f_jlog, c.f_zlog, c.b_log):
         sent(r.log_in.at[pl.ds(0, 7)], channel)
 
 

time: 108 us -> 107 us (level)
  no operation moved by 1% of the time
where the time goes in v4:
time: 107 us
  Pallas kernels  106 us (99%)
    pallas_call x1, Pallas kernels, shards(): pl.pallas_call(kernel, out_shape=arrays, in_specs=[pl.BlockSpec(memory_sp...  104 us
    pallas_call x1, Pallas kernels, shards(): pl.pallas_call(publish, out_shape=arrays, in_specs=[pl.BlockSpec(memory_s...  2.31 us

profile of v4, /device:TPU:1, one launch (start us, length us, event | category | flops | bytes accessed | tf_op | source)
XLA Modules:
  0.0 107.1 jit_solution(1049394658970107566)
XLA Ops:
  0.6 104.2 %layer_backward.1 = (bf16[2048,256]{1,0:T(8,128)(2,1)S(1)}, bf16[2048,256]{1,0:T(8,128)(2,1)S(1)}, bf16[256,2048]{1,0:T(8,128)(2,1)S(1)}, f32[32,1024]{1,0:T(8,1...) custom-call(bf16[128,2048]{1,0:T(8,128)(2,1)} %refs_0_.1, ...), custom_call_target="tpu_custom_call" | custom-call | tf_op jit(solution)/shard_map/layer_backward/pallas_call | solution.py:936
  104.8 2.3 %publish.1 = (bf16[2048,256]{1,0:T(8,128)(2,1)}, bf16[2048,256]{1,0:T(8,128)(2,1)}, bf16[256,2048]{1,0:T(8,128)(2,1)}, f32[32,1024]{1,0:T(8,128)}, f32[128,512]{...) custom-call(bf16[2048,256]{1,0:T(8,128)(2,1)S(1)} %get-tuple-element, ...), custom_call_target="tpu_custom_call" | custom-call | tf_op jit(solution)/shard_map/publish/pallas_call | solution.py:947

commit v5 on v4

--- a/solution.py
+++ b/solution.py
@@ -766,16 +766,14 @@
 
     r.b_in[j] = r.b_own[j]
 
-    mixed_ring.near()
-    share(mixed_ring, c.mixed_c, mixed_ring.left, mixed_ring.right)
-
     got(r.b_in.at[pl.ds(0, 7)], c.b_j)
     carry_group(r.b_in, r.b_run, True)
     across_planes(r.b_run, r.b_z, c.b_z)
     to_group(r.before, r.b_group, c.b_group)
     to_group(r.log_before, r.b_log, c.b_log)
+    mixed_ring.near()
     mixed_ring.far()
-    share(mixed_ring, c.mixed_c, mixed_ring.opp)
+    share(mixed_ring, c.mixed_c, mixed_ring.left, mixed_ring.right, mixed_ring.opp)
 
     columns_ring.near()
     columns_ring.far()

time: 107 us -> 107 us (level)
  no operation moved by 1% of the time
where the time goes in v5:
time: 107 us
  Pallas kernels  106 us (99%)
    pallas_call x1, Pallas kernels, shards(): pl.pallas_call(kernel, out_shape=arrays, in_specs=[pl.BlockSpec(memory_sp...  104 us
    pallas_call x1, Pallas kernels, shards(): pl.pallas_call(publish, out_shape=arrays, in_specs=[pl.BlockSpec(memory_s...  2.31 us

profile of v5, /device:TPU:1, one launch (start us, length us, event | category | flops | bytes accessed | tf_op | source)
XLA Modules:
  0.0 106.6 jit_solution(6642276425755064967)
XLA Ops:
  0.6 103.6 %layer_backward.1 = (bf16[2048,256]{1,0:T(8,128)(2,1)S(1)}, bf16[2048,256]{1,0:T(8,128)(2,1)S(1)}, bf16[256,2048]{1,0:T(8,128)(2,1)S(1)}, f32[32,1024]{1,0:T(8,1...) custom-call(bf16[128,2048]{1,0:T(8,128)(2,1)} %refs_0_.1, ...), custom_call_target="tpu_custom_call" | custom-call | tf_op jit(solution)/shard_map/layer_backward/pallas_call | solution.py:934
  104.3 2.3 %publish.1 = (bf16[2048,256]{1,0:T(8,128)(2,1)}, bf16[2048,256]{1,0:T(8,128)(2,1)}, bf16[256,2048]{1,0:T(8,128)(2,1)}, f32[32,1024]{1,0:T(8,128)}, f32[128,512]{...) custom-call(bf16[2048,256]{1,0:T(8,128)(2,1)S(1)} %get-tuple-element, ...), custom_call_target="tpu_custom_call" | custom-call | tf_op jit(solution)/shard_map/publish/pallas_call | solution.py:945

commit v6 on v5

--- a/solution.py
+++ b/solution.py
@@ -226,9 +226,10 @@
 
     barrier = pltpu.get_barrier_semaphore()
 
-    @pl.loop(1, 64)
-    def _(d):
-        peer = (me + d) % 64
+    @pl.loop(0, 63)
+    def _(n):
+        away = (n // 2 + 1) * (1 - 2 * (n % 2))
+        peer = (me + 32 + away * (1 - n // 62)) % 64
         pl.semaphore_signal(barrier, inc=1, device_id=(peer, tx), device_id_type=MESH)
 
     for side in (right, left, opp):

time: 107 us -> 108 us (level)
  no operation moved by 1% of the time
where the time goes in v6:
time: 108 us
  Pallas kernels  107 us (99%)
    pallas_call x1, Pallas kernels, shards(): pl.pallas_call(kernel, out_shape=arrays, in_specs=[pl.BlockSpec(memory_sp...  105 us
    pallas_call x1, Pallas kernels, shards(): pl.pallas_call(publish, out_shape=arrays, in_specs=[pl.BlockSpec(memory_s...  2.31 us

profile of v6, /device:TPU:1, one launch (start us, length us, event | category | flops | bytes accessed | tf_op | source)
XLA Modules:
  0.0 107.5 jit_solution(3350170197550699883)
XLA Ops:
  0.6 104.5 %layer_backward.1 = (bf16[2048,256]{1,0:T(8,128)(2,1)S(1)}, bf16[2048,256]{1,0:T(8,128)(2,1)S(1)}, bf16[256,2048]{1,0:T(8,128)(2,1)S(1)}, f32[32,1024]{1,0:T(8,1...) custom-call(bf16[128,2048]{1,0:T(8,128)(2,1)} %refs_0_.1, ...), custom_call_target="tpu_custom_call" | custom-call | tf_op jit(solution)/shard_map/layer_backward/pallas_call | solution.py:935
  105.2 2.3 %publish.1 = (bf16[2048,256]{1,0:T(8,128)(2,1)}, bf16[2048,256]{1,0:T(8,128)(2,1)}, bf16[256,2048]{1,0:T(8,128)(2,1)}, f32[32,1024]{1,0:T(8,128)}, f32[128,512]{...) custom-call(bf16[2048,256]{1,0:T(8,128)(2,1)S(1)} %get-tuple-element, ...), custom_call_target="tpu_custom_call" | custom-call | tf_op jit(solution)/shard_map/publish/pallas_call | solution.py:946
